TPU v7x, 32 devices: a whole 2x2x4 slice. The times are simulated.
32 devices in a mesh: rep: 2 (over x), fs: 8 (over z, y), tp: 2 (over core).
Axes of the slice: x: 2, y: 2, z: 4, core: 2. Of those that a mesh axis runs over, the one named last changes fastest.
Arguments:
- stream: bfloat16 [6144, 2048], P(('rep', 'fs'), 'tp'), may hold values from -24 to 24
- recurrence_input_weight: bfloat16 [2048, 2048], P('fs', 'tp'), may hold values from -0.125 to 0.125
- output_gate_weight: bfloat16 [2048, 2048], P('fs', 'tp'), may hold values from -0.125 to 0.125
- recurrence_gate_matrix: bfloat16 [16, 128, 128], P('tp'), may hold values from -0.5 to 0.5
- input_gate_matrix: bfloat16 [16, 128, 128], P('tp'), may hold values from -0.5 to 0.5
- channel_decay_rate: float32 [2048], P('tp')
- recurrence_taps: float32 [4, 2048], P(None, 'tp'), may hold values from -3 to 3
- spike_log_decay: float32 [6144, 16], P(('rep', 'fs'), 'tp'), may hold values from -2.1 to 0
- recurrence_output_weight: bfloat16 [2048, 2048], P('tp', 'fs'), may hold values from -0.3125 to 0.3125
- feedforward_gate_upward: bfloat16 [2048, 4096], P('fs', 'tp'), may hold values from -0.125 to 0.125
- feedforward_value_upward: bfloat16 [2048, 4096], P('fs', 'tp'), may hold values from -0.125 to 0.125
- feedforward_gate_taps: float32 [3, 4096], P(None, 'tp'), may hold values from -3 to 3
- feedforward_value_taps: float32 [3, 4096], P(None, 'tp'), may hold values from -3 to 3
- feedforward_down_weight: bfloat16 [4096, 2048], P('tp', 'fs'), may hold values from -0.1875 to 0.1875
- recurrence_norm_gain: float32 [2048], replicated, may hold values from 0.1 to 1.9
- feedforward_norm_gain: float32 [2048], replicated, may hold values from 0.1 to 1.9
- closing_norm_gain: float32 [2048], replicated, may hold values from 0.1 to 1.9
Outputs:
- layer_out: bfloat16 [6144, 2048], P(('rep', 'fs'), 'tp')
All inputs are finite; a program needn't handle non-finite values.
Results may differ from a plain program's by a relative error of at most 0.018.
Values may be sent and summed in bfloat16 or wider, within the bound.
A program may use at most 64 MiB of HBM per device.

v0:
```python
import functools

import jax
import jax.numpy as jnp
from jax import lax
from jax.experimental import pallas as pl
from jax.experimental.pallas import tpu as pltpu
from jax.sharding import PartitionSpec as P

EPS = 1e-06
GATE_POWER = 8.0


def rms_scale(row_block, gain_vec):
    widened = row_block.astype(jnp.float32)
    inverse = lax.rsqrt(jnp.mean(widened * widened, axis=-1, keepdims=True) + EPS)
    return (widened * inverse * gain_vec).astype(jnp.bfloat16)


def causal_mix(values, kernel_taps):
    extent = kernel_taps.shape[0]
    length = values.shape[0]
    padded = jnp.pad(values, ((extent - 1, 0), (0, 0)))
    summed = kernel_taps[0] * padded[0:length]
    for offset in range(1, extent):
        summed = summed + kernel_taps[offset] * padded[offset : offset + length]
    return summed


def chain_step(earlier, following):
    return (earlier[0] * following[0], following[0] * earlier[1] + following[1])


def fold_pair(source, pieces):
    return (
        jnp.dot(source, pieces[0], preferred_element_type=jnp.float32),
        jnp.dot(source, pieces[1], preferred_element_type=jnp.float32),
    )


def project_with(left_rows, weight_piece):
    return jnp.dot(left_rows, weight_piece, preferred_element_type=jnp.float32).astype(jnp.bfloat16)


def third_rows(rows):
    return rows // 3 // 16 * 16


class RingGather:
    def __init__(self, n, sources, targets, send_sems, recv_sems):
        self.n = n
        self.sources = sources
        self.targets = targets
        self.send_sems = send_sems
        self.recv_sems = recv_sems
        self.rep = lax.axis_index("rep")
        fs = lax.axis_index("fs")
        self.fs = fs
        side = lax.rem(fs, 2)
        depth = fs // 2
        self.place = depth + side * (n - 1 - 2 * depth)

    def member(self, shift):
        place = lax.rem(self.place + shift + 2 * self.n, self.n)
        side = place // (self.n // 2)
        depth = place + side * (self.n - 1 - 2 * place)
        return 2 * depth + side

    def neighbours(self):
        return (
            {"fs": self.member(1)},
            {"fs": self.member(-1)},
            {"rep": 1 - self.rep},
            {"tp": 1 - lax.axis_index("tp")},
        )

    def enter(self):
        barrier = pltpu.get_barrier_semaphore()
        for device in self.neighbours():
            pl.semaphore_signal(
                barrier, inc=1, device_id=device, device_id_type=pl.DeviceIdType.MESH
            )
        pl.semaphore_wait(barrier, 4)

    def piece(self, ref, w, lane, base, other=False):
        rows = self.sources[w].shape[0]
        part = third_rows(rows)
        if lane == 1:
            return ref.at[pl.ds(pl.multiple_of(base + part, 16), rows - 2 * part), :]
        rep = 1 - self.rep if other else self.rep
        return ref.at[pl.ds(pl.multiple_of(base + rep * (rows - part), 16), part), :]

    def heading(self, w, lane):
        return 1 if (w + lane) % 2 == 0 else -1

    def copy(self, w, lane, step, source, target, device):
        return pltpu.make_async_remote_copy(
            src_ref=source,
            dst_ref=target,
            send_sem=self.send_sems.at[w, lane, step],
            recv_sem=self.recv_sems.at[w, lane, step],
            device_id=device,
            device_id_type=pl.DeviceIdType.MESH,
        )

    def hop(self, w, lane, step):
        way = self.heading(w, lane)
        base = self.member(-way * step) * self.sources[w].shape[0]
        target = self.piece(self.targets[w], w, lane, base)
        source = self.piece(self.sources[w], w, lane, 0) if step == 0 else target
        return self.copy(w, lane, step, source, target, {"fs": self.member(way)})

    def arrival(self, w, lane, step):
        way = self.heading(w, lane)
        base = self.member(-way * (step + 1)) * self.sources[w].shape[0]
        target = self.piece(self.targets[w], w, lane, base)
        return self.copy(w, lane, step, target, target, {"fs": self.member(way)})

    def cross(self, w, step, other=False):
        way = self.heading(w, 0)
        if other:
            way_base = self.member(-way * (step + 1)) * self.sources[w].shape[0]
            target = self.piece(self.targets[w], w, 0, way_base, other=True)
        else:
            way_base = self.member(-way * (step + 1)) * self.sources[w].shape[0]
            target = self.piece(self.targets[w], w, 0, way_base)
        return self.copy(w, 2, step, target, target, {"rep": 1 - self.rep})

    def local(self, w, sem):
        rows = self.sources[w].shape[0]
        own = self.targets[w].at[pl.ds(pl.multiple_of(self.fs * rows, 16), rows), :]
        return pltpu.make_async_copy(self.sources[w], own, sem.at[w])

    def start(self, w):
        for lane in (0, 1):
            self.hop(w, lane, 0).start()

    def serve(self, w, step):
        for lane in (0, 1):
            self.arrival(w, lane, step).wait_recv()
            if step + 1 < self.n - 1:
                self.hop(w, lane, step + 1).start()
            if lane == 0:
                self.cross(w, step).start()

    def crossed(self, w):
        for step in range(self.n - 1):
            self.cross(w, step, other=True).wait_recv()

    def drain(self, w):
        for step in range(self.n - 1):
            self.hop(w, 0, step).wait_send()
            self.hop(w, 1, step).wait_send()
            self.cross(w, step).wait_send()


def gelu_of(x):
    return 0.5 * x * (1.0 + jnp.tanh(0.7978845608028654 * (x + 0.044715 * (x * x * x))))


def one_less_exp(z):
    series = 1.0 + z * (1.0 / 6.0)
    for order in (5.0, 4.0, 3.0, 2.0):
        series = 1.0 + z * (1.0 / order) * series
    return jnp.where(z > -0.35, -z * series, 1.0 - jnp.exp(z))


def tap_rows(values, taps_ref, cols):
    extent = taps_ref.shape[0]
    summed = taps_ref[extent - 1 : extent, cols] * values
    row = lax.broadcasted_iota(jnp.int32, values.shape, 0)
    for back in range(1, extent):
        moved = jnp.where(row >= back, pltpu.roll(values, back, 0), 0.0)
        summed = summed + taps_ref[extent - 1 - back : extent - back, cols] * moved
    return summed


def dot32(a, b):
    return jnp.dot(a, b, preferred_element_type=jnp.float32)


def layer_kernel(n, *refs):
    sources = refs[:6]
    (stream, reset_map, admit_map, decay_base, taps, spike) = refs[6:12]
    (gate_taps, value_taps, rec_gain, ffn_gain, last_gain, out) = refs[12:18]
    targets = refs[18:24]
    (stream_in, normed, gate_src, decay, inflow, mixed) = refs[24:30]
    (away, landed, kept, middle, middle_in, hidden, final, sums, sums_in) = refs[30:39]
    local_sems, send_sems, recv_sems, pair_send, pair_recv = refs[39:]
    tokens, width = stream.shape
    me = lax.axis_index("tp")
    ring = RingGather(n, sources, targets, send_sems, recv_sems)
    bf16, f32 = jnp.bfloat16, jnp.float32
    tile = 256
    strip = 48

    def pair(i, source, target):
        return pltpu.make_async_remote_copy(
            src_ref=source,
            dst_ref=target,
            send_sem=pair_send.at[i],
            recv_sem=pair_recv.at[i],
            device_id={"tp": 1 - me},
            device_id_type=pl.DeviceIdType.MESH,
        )

    def half(which):
        return pl.ds(pl.multiple_of(which * width, 128), width)

    def strips(body):
        def step(i, carry):
            body(pl.ds(pl.multiple_of(i * strip, 16), strip))
            return carry

        lax.fori_loop(0, tokens // strip, step, 0)

    def norm_into(mine, theirs, gain):
        def body(rows):
            a = mine[rows, :].astype(f32)
            b = theirs[rows, :].astype(f32)
            total = jnp.sum(a * a, axis=1, keepdims=True) + jnp.sum(b * b, axis=1, keepdims=True)
            inverse = lax.rsqrt(total * (1.0 / (2 * width)) + EPS)
            normed[rows, half(me)] = (a * inverse * gain[:, half(me)]).astype(bf16)
            normed[rows, half(1 - me)] = (b * inverse * gain[:, half(1 - me)]).astype(bf16)

        strips(body)

    def project(i, rows, w):
        depth = rows.shape[1]
        per_half = n // 2

        def into(target, which):
            def step(j, carry):
                slot = which * per_half + j
                block = targets[w][pl.ds(pl.multiple_of(slot * depth, 16), depth), :]
                cols = pl.ds(pl.multiple_of(j * tile, 128), tile)
                target[:, cols] = dot32(rows[...], block).astype(bf16)
                return carry

            lax.fori_loop(0, per_half, step, 0)

        into(away.at[i], 1 - me)
        sent = pair(1 + i, away.at[i], landed.at[i])
        sent.start()
        into(kept, me)
        sent.wait()

    def ready(w):
        ring.local(w, local_sems).wait()
        ring.crossed(w)

    ring.enter()
    first = pair(0, stream, stream_in)
    first.start()
    for w in range(3):
        ring.start(w)
    for w in range(6):
        ring.local(w, local_sems).start()
    first.wait()
    norm_into(stream, stream_in, rec_gain)
    for step in range(n - 1):
        for w in range(3):
            ring.serve(w, step)
        if step == n - 3:
            ring.start(3)
            ring.start(4)
    for w in range(3):
        ready(w)

    def ticks(step):
        ring.serve(3, step)
        ring.serve(4, step)

    for c in range(width // tile):
        cols = slice(c * tile, (c + 1) * tile)
        rec = dot32(normed[...], targets[0][:, cols]).astype(bf16).astype(f32)
        conv = tap_rows(rec, taps, cols).astype(bf16)
        gate_src[:, cols] = dot32(normed[...], targets[1][:, cols]).astype(bf16)
        for part in range(tile // 128):
            h = c * (tile // 128) + part
            lanes = slice(h * 128, (h + 1) * 128)
            block = conv[:, part * 128 : (part + 1) * 128]
            reset = jax.nn.sigmoid(dot32(block, reset_map[h]))
            admit = jax.nn.sigmoid(dot32(block, admit_map[h]))
            log_decay = spike[:, h : h + 1] - reset * decay_base[:, lanes]
            decay[:, lanes] = jnp.exp(log_decay)
            inflow[:, lanes] = jnp.sqrt(one_less_exp(2.0 * log_decay)) * admit * block.astype(f32)
        ticks(c)

    ring.start(5)
    row = lax.broadcasted_iota(jnp.int32, (8, width), 0)

    def scan_step(i, carry):
        rows = pl.ds(pl.multiple_of(i * 16, 16), 16)
        a16, b16 = decay[rows, :], inflow[rows, :]
        found = []
        for part in range(2):
            a, b = a16[part * 8 : part * 8 + 8], b16[part * 8 : part * 8 + 8]
            for back in (1, 2, 4):
                a_before = jnp.where(row >= back, pltpu.roll(a, back, 0), 1.0)
                b_before = jnp.where(row >= back, pltpu.roll(b, back, 0), 0.0)
                b = a * b_before + b
                a = a * a_before
            states = a * carry + b
            carry = states[7:8, :]
            found.append(states)
        states = jnp.concatenate(found, axis=0)
        mixed[rows, :] = (states * gelu_of(gate_src[rows, :].astype(f32))).astype(bf16)
        return carry

    lax.fori_loop(0, tokens // 16, scan_step, jnp.zeros((1, width), f32))
    served = width // tile
    ticks(served)
    project(0, mixed, 2)

    def add_branch(rows):
        branch = (kept[rows, :].astype(f32) + landed[0, rows, :].astype(f32)).astype(bf16)
        middle[rows, :] = (stream[rows, :].astype(f32) + branch.astype(f32)).astype(bf16)

    strips(add_branch)
    shared = pair(3, middle, middle_in)
    shared.start()
    shared.wait()
    for step in range(served + 1, n - 1):
        ticks(step)
        if step == served + 1:
            norm_into(middle, middle_in, ffn_gain)
    ready(3)
    ready(4)

    def up_step(t, carry):
        cols = pl.ds(pl.multiple_of(t * tile, 128), tile)
        gate = dot32(normed[...], targets[3][:, cols]).astype(bf16).astype(f32)
        gate = gelu_of(tap_rows(gate, gate_taps, cols))
        value = dot32(normed[...], targets[4][:, cols]).astype(bf16).astype(f32)
        hidden[:, cols] = (gate * tap_rows(value, value_taps, cols)).astype(bf16)
        return carry

    tiles = hidden.shape[1] // tile
    for step in range(n - 1):
        lax.fori_loop(step * tiles // (n - 1), (step + 1) * tiles // (n - 1), up_step, 0)
        ring.serve(5, step)
    ready(5)
    project(1, hidden, 5)

    def finish(rows):
        branch = (kept[rows, :].astype(f32) + landed[1, rows, :].astype(f32)).astype(bf16)
        total = middle[rows, :].astype(f32) + branch.astype(f32)
        final[rows, :] = total
        square = jnp.sum(total * total, axis=1, keepdims=True)
        sums[rows, :] = jnp.broadcast_to(square, (strip, 128))

    strips(finish)
    summed = pair(4, sums, sums_in)
    summed.start()
    summed.wait()

    def scale(rows):
        square = sums[rows, :] + sums_in[rows, :]
        inverse = lax.rsqrt(square * (1.0 / (2 * width)) + EPS)[:, 0:1]
        out[rows, :] = (final[rows, :] * inverse * last_gain[:, half(me)]).astype(bf16)

    strips(scale)
    for w in range(6):
        ring.drain(w)


def fused_layer(n, weights, others):
    tokens, width = others[0].shape
    wide = weights[3].shape[1]
    bf16, f32 = jnp.bfloat16, jnp.float32
    vmem = pltpu.VMEM
    return pl.pallas_call(
        functools.partial(layer_kernel, n),
        out_shape=jax.ShapeDtypeStruct((tokens, width), bf16),
        in_specs=[pl.BlockSpec(memory_space=pl.ANY)] * 6
        + [pl.BlockSpec(memory_space=vmem)] * len(others),
        out_specs=pl.BlockSpec(memory_space=vmem),
        scratch_shapes=[vmem((n * w.shape[0], w.shape[1]), w.dtype) for w in weights]
        + [
            vmem((tokens, width), bf16),
            vmem((tokens, 2 * width), bf16),
            vmem((tokens, width), bf16),
            vmem((tokens, width), f32),
            vmem((tokens, width), f32),
            vmem((tokens, width), bf16),
            vmem((2, tokens, width), bf16),
            vmem((2, tokens, width), bf16),
            vmem((tokens, width), bf16),
            vmem((tokens, width), bf16),
            vmem((tokens, width), bf16),
            vmem((tokens, wide), bf16),
            vmem((tokens, width), f32),
            vmem((tokens, 128), f32),
            vmem((tokens, 128), f32),
            pltpu.SemaphoreType.DMA((6,)),
            pltpu.SemaphoreType.DMA((6, 3, n - 1)),
            pltpu.SemaphoreType.DMA((6, 3, n - 1)),
            pltpu.SemaphoreType.DMA((5,)),
            pltpu.SemaphoreType.DMA((5,)),
        ],
        compiler_params=pltpu.CompilerParams(
            collective_id=0, has_side_effects=True, vmem_limit_bytes=66_000_000
        ),
    )(*weights, *others)


def shards(
    ringed,
    stream,
    recurrence_input_weight,
    output_gate_weight,
    recurrence_gate_matrix,
    input_gate_matrix,
    channel_decay_rate,
    recurrence_taps,
    spike_log_decay,
    recurrence_output_weight,
    feedforward_gate_upward,
    feedforward_value_upward,
    feedforward_gate_taps,
    feedforward_value_taps,
    feedforward_down_weight,
    recurrence_norm_gain,
    feedforward_norm_gain,
    closing_norm_gain,
):
    tok_rows = stream.shape[0]
    fs_size = lax.axis_size("fs")
    if ringed:
        return fused_layer(
            fs_size,
            (
                recurrence_input_weight,
                output_gate_weight,
                recurrence_output_weight,
                feedforward_gate_upward,
                feedforward_value_upward,
                feedforward_down_weight,
            ),
            (
                stream,
                recurrence_gate_matrix,
                input_gate_matrix,
                (GATE_POWER * jax.nn.softplus(-channel_decay_rate))[None, :],
                recurrence_taps,
                spike_log_decay,
                feedforward_gate_taps,
                feedforward_value_taps,
                recurrence_norm_gain[None, :],
                feedforward_norm_gain[None, :],
                closing_norm_gain[None, :],
            ),
        )
    weights = [
        lax.all_gather(recurrence_input_weight, "fs", axis=0, tiled=True),
        lax.all_gather(output_gate_weight, "fs", axis=0, tiled=True),
        lax.all_gather(recurrence_output_weight, "fs", axis=1, tiled=True),
        lax.all_gather(feedforward_gate_upward, "fs", axis=0, tiled=True),
        lax.all_gather(feedforward_value_upward, "fs", axis=0, tiled=True),
        lax.all_gather(feedforward_down_weight, "fs", axis=1, tiled=True),
    ]
    head_count = recurrence_gate_matrix.shape[0]
    block_size = recurrence_gate_matrix.shape[1]
    whole_rows = lax.all_gather(stream, "tp", axis=1, tiled=True)
    normed = rms_scale(whole_rows, recurrence_norm_gain)
    rec_sum, gate_sum = fold_pair(
        normed,
        (
            weights[0],
            weights[1],
        ),
    )
    rec_in = rec_sum.astype(jnp.bfloat16)
    gate_src = gate_sum.astype(jnp.bfloat16)
    conv_out = causal_mix(rec_in.astype(jnp.float32), recurrence_taps).astype(jnp.bfloat16)
    blocks = conv_out.reshape(tok_rows, head_count, block_size)
    gate_restart = jax.nn.sigmoid(
        jnp.einsum(
            "thi,hij->thj", blocks, recurrence_gate_matrix, preferred_element_type=jnp.float32
        )
    )
    admit_gate = jax.nn.sigmoid(
        jnp.einsum("thi,hij->thj", blocks, input_gate_matrix, preferred_element_type=jnp.float32)
    )
    decay_base = (GATE_POWER * jax.nn.softplus(-channel_decay_rate)).reshape(head_count, block_size)
    decay_logarithm = -gate_restart * decay_base + spike_log_decay[:, :, None]
    decay_rate = jnp.exp(decay_logarithm)
    inflow = jnp.sqrt(-jnp.expm1(2.0 * decay_logarithm)) * admit_gate * blocks.astype(jnp.float32)
    states = lax.associative_scan(chain_step, (decay_rate, inflow), axis=0)[1]
    mixed_out = (
        states.reshape(tok_rows, head_count * block_size)
        * jax.nn.gelu(gate_src.astype(jnp.float32))
    ).astype(jnp.bfloat16)
    mix_terms = project_with(
        mixed_out, weights[2]
    )
    branch = lax.psum_scatter(
        lax.optimization_barrier(mix_terms).astype(jnp.float32).astype(jnp.bfloat16),
        "tp",
        scatter_dimension=1,
        tiled=True,
    )
    middle = (stream.astype(jnp.float32) + branch.astype(jnp.float32)).astype(jnp.bfloat16)
    whole_middle = lax.all_gather(middle, "tp", axis=1, tiled=True)
    normed_ffn = rms_scale(whole_middle, feedforward_norm_gain)
    gate_sum_ffn, value_sum_ffn = fold_pair(
        normed_ffn,
        (
            weights[3],
            weights[4],
        ),
    )
    gate_up = gate_sum_ffn.astype(jnp.bfloat16)
    value_up = value_sum_ffn.astype(jnp.bfloat16)
    gate_conv = causal_mix(gate_up.astype(jnp.float32), feedforward_gate_taps)
    value_conv = causal_mix(value_up.astype(jnp.float32), feedforward_value_taps)
    hidden = (jax.nn.gelu(gate_conv) * value_conv).astype(jnp.bfloat16)
    down_terms = project_with(
        hidden, weights[5]
    )
    branch_ffn = lax.psum_scatter(
        lax.optimization_barrier(down_terms).astype(jnp.float32).astype(jnp.bfloat16),
        "tp",
        scatter_dimension=1,
        tiled=True,
    )
    final_rows = middle.astype(jnp.float32) + branch_ffn.astype(jnp.float32)
    col_count = final_rows.shape[1]
    square_sum = lax.psum(jnp.sum(final_rows * final_rows, axis=1), "tp")
    inverse = lax.rsqrt(square_sum / (col_count * lax.axis_size("tp")) + EPS)
    gain_part = lax.dynamic_slice_in_dim(
        closing_norm_gain, lax.axis_index("tp") * col_count, col_count
    )
    return (final_rows * inverse[:, None] * gain_part[None, :]).astype(jnp.bfloat16)


def solution(mesh):
    in_specs = (
        P(("rep", "fs"), "tp"),
        P("fs", "tp"),
        P("fs", "tp"),
        P("tp", None, None),
        P("tp", None, None),
        P("tp"),
        P(None, "tp"),
        P(("rep", "fs"), "tp"),
        P("tp", "fs"),
        P("fs", "tp"),
        P("fs", "tp"),
        P(None, "tp"),
        P(None, "tp"),
        P("tp", "fs"),
        P(),
        P(),
        P(),
    )
    out_specs = P(("rep", "fs"), "tp")
    ringed = mesh.shape["rep"] == 2 and mesh.shape["tp"] == 2 and mesh.shape["fs"] == 8
    body = functools.partial(shards, ringed)
    return jax.shard_map(body, mesh=mesh, in_specs=in_specs, out_specs=out_specs, check_vma=False)
```

profile of v0, /device:TPU:0, one launch (start us, length us, event | category | flops | bytes accessed | tf_op | source)
XLA Modules:
  0.0 285.2 jit_solution(11361976878402811949)
XLA Ops:
  0.0 0.0 copy-start
  0.0 1.3 fusion
  1.3 0.0 copy-done
  1.3 0.8 copy.18.refs_11_
  2.1 281.0 %shard_map.163 = bf16[384,1024]{1,0:T(8,128)(2,1)} custom-call(bf16[256,1024]{1,0:T(8,128)(2,1)} %refs_0_.1, bf16[256,1024]{1,0:T(8,128)(2,1)} %refs_1_.1, bf16[1024,256]{1,0:T(8,128)(2,1)} %refs_2_.1, bf16[256,2048]{1,0:T(8,128)(2,1)} %refs_3_.1, bf16[256,2048]{1,0:T(8,128)(2,1)} %refs_4_.1, bf16[2048,256]{1,0:T(8,128)(2,1)} %refs_5_.1, ...), custom_call_target="tpu_custom_call" | custom-call | tf_op jit(solution)/shard_map/pallas_call | solution.py:373
  283.2 2.1 copy.20
Async XLA Ops:
  0.0 1.3 copy-start
where the time goes:
time: 285 us
  Pallas kernels  281 us (99%)
  local copies, waits for them, and re-layouts  2.88 us (1%)
    pallas_call x1, Pallas kernels, fused_layer(): pl.pallas_call(functools.partial(layer_kernel, n), out_shape=jax.ShapeDty...  281 us

commit v1 on v0

v1 whole, which is shorter than its diff:
```python
import functools

import jax
import jax.numpy as jnp
from jax import lax
from jax.experimental import pallas as pl
from jax.experimental.pallas import tpu as pltpu
from jax.sharding import PartitionSpec as P

EPS = 1e-06
GATE_POWER = 8.0


def rms_scale(row_block, gain_vec):
    widened = row_block.astype(jnp.float32)
    inverse = lax.rsqrt(jnp.mean(widened * widened, axis=-1, keepdims=True) + EPS)
    return (widened * inverse * gain_vec).astype(jnp.bfloat16)


def causal_mix(values, kernel_taps):
    extent = kernel_taps.shape[0]
    length = values.shape[0]
    padded = jnp.pad(values, ((extent - 1, 0), (0, 0)))
    summed = kernel_taps[0] * padded[0:length]
    for offset in range(1, extent):
        summed = summed + kernel_taps[offset] * padded[offset : offset + length]
    return summed


def chain_step(earlier, following):
    return (earlier[0] * following[0], following[0] * earlier[1] + following[1])


def fold_pair(source, pieces):
    return (
        jnp.dot(source, pieces[0], preferred_element_type=jnp.float32),
        jnp.dot(source, pieces[1], preferred_element_type=jnp.float32),
    )


def project_with(left_rows, weight_piece):
    return jnp.dot(left_rows, weight_piece, preferred_element_type=jnp.float32).astype(jnp.bfloat16)


class PairGather:
    def __init__(self, n, sources, targets, sems):
        self.n = n
        self.sources = sources
        self.targets = targets
        (self.local_sem, self.y_send, self.y_recv, self.z_send, self.z_recv, self.x_send, self.x_recv) = sems
        self.x = lax.axis_index("rep")
        fs = lax.axis_index("fs")
        self.y = lax.rem(fs, 2)
        self.z = fs // 2
        self.inner = jnp.logical_and(self.z > 0, self.z < n // 2 - 1)

    def level(self, k):
        if k == 0:
            return self.z
        if k == 1:
            return self.z + 1 - 2 * lax.rem(self.z, 2)
        if k == 2:
            return lax.rem(self.z + 2, 4)
        return 3 - self.z

    def side(self, q):
        return lax.rem(self.y + q, 2)

    def member(self, k, q):
        return 2 * self.level(k) + self.side(q)

    def enter(self):
        barrier = pltpu.get_barrier_semaphore()
        devices = [
            {"rep": 1 - self.x},
            {"tp": 1 - lax.axis_index("tp")},
            {"fs": self.member(0, 1)},
            {"fs": self.member(1, 0)},
            {"fs": self.member(2, 0)},
            {"fs": self.member(3, 0)},
        ]
        for device in devices:
            pl.semaphore_signal(
                barrier, inc=1, device_id=device, device_id_type=pl.DeviceIdType.MESH
            )
        pl.semaphore_wait(barrier, len(devices))

    def depth(self, w):
        return self.targets[w].shape[0] // self.n

    def source(self, w, half, r):
        ref, depth = self.sources[w], self.depth(w)
        part = depth // 2
        cols = self.targets[w].shape[1]
        if ref.shape[0] == depth:
            return ref.at[
                pl.ds(pl.multiple_of(r * part, 16), part),
                pl.ds(pl.multiple_of(half * cols, 128), cols),
            ]
        return ref.at[pl.ds(pl.multiple_of(half * depth + r * part, 16), part), :]

    def piece(self, w, shard, r):
        depth = self.depth(w)
        part = depth // 2
        return self.targets[w].at[pl.ds(pl.multiple_of(shard * depth + r * part, 16), part), :]

    def copy(self, source, target, send_sem, recv_sem, device):
        return pltpu.make_async_remote_copy(
            src_ref=source,
            dst_ref=target,
            send_sem=send_sem,
            recv_sem=recv_sem,
            device_id=device,
            device_id_type=pl.DeviceIdType.MESH,
        )

    def local(self, w, r):
        return pltpu.make_async_copy(
            self.source(w, self.y, r), self.piece(w, self.member(0, 0), r), self.local_sem.at[w, r]
        )

    def half_of(self, i):
        return self.x if i == 0 else 1 - self.x

    def y_copy(self, w, i):
        r = self.half_of(i)
        return self.copy(
            self.source(w, 1 - self.y, r),
            self.piece(w, self.member(0, 0), r),
            self.y_send.at[w, i],
            self.y_recv.at[w, i],
            {"fs": self.member(0, 1)},
        )

    def y_arrival(self, w, i):
        target = self.piece(w, self.member(0, 1), self.half_of(i))
        return self.copy(
            target, target, self.y_send.at[w, i], self.y_recv.at[w, i], {"fs": self.member(0, 1)}
        )

    def z_copy(self, w, q, k):
        target = self.piece(w, self.member(0, q), self.x)
        source = self.source(w, self.y, self.x) if q == 0 else target
        return self.copy(
            source,
            target,
            self.z_send.at[w, q, k],
            self.z_recv.at[w, q, k],
            {"fs": self.member(k, 0)},
        )

    def z_arrival(self, w, q, k):
        target = self.piece(w, self.member(k, q), self.x)
        return self.copy(
            target,
            target,
            self.z_send.at[w, q, k],
            self.z_recv.at[w, q, k],
            {"fs": self.member(k, 0)},
        )

    def z_forward(self, w, q):
        target = self.piece(w, self.member(2, q), self.x)
        return self.copy(
            target,
            target,
            self.z_send.at[w, q, 0],
            self.z_recv.at[w, q, 3],
            {"fs": self.member(1, 0)},
        )

    def x_copy(self, w, q, k):
        target = self.piece(w, self.member(k, q), self.x)
        return self.copy(
            target, target, self.x_send.at[w, q, k], self.x_recv.at[w, q, k], {"rep": 1 - self.x}
        )

    def x_arrival(self, w, q, k):
        target = self.piece(w, self.member(k, q), 1 - self.x)
        return self.copy(
            target, target, self.x_send.at[w, q, k], self.x_recv.at[w, q, k], {"rep": 1 - self.x}
        )

    def z_start(self, w, q):
        for k in (2, 1):
            self.z_copy(w, q, k).start()

        @pl.when(self.inner)
        def _():
            self.z_copy(w, q, 3).start()

    def cross(self, w):
        self.y_arrival(w, 0).wait_recv()
        self.z_start(w, 1)

    def serve(self, w, q, k):
        self.z_arrival(w, q, k).wait_recv()
        if k == 2:

            @pl.when(self.inner)
            def _():
                self.z_forward(w, q).start()

        self.x_copy(w, q, k).start()

    def own_ready(self, w):
        for r in (0, 1):
            self.local(w, r).wait()
        self.y_arrival(w, 1).wait_recv()

    def ready(self, w):
        self.own_ready(w)
        for q in (0, 1):
            for k in (1, 2, 3):
                self.x_arrival(w, q, k).wait_recv()

    def drain(self, w):
        for i in (0, 1):
            self.y_copy(w, i).wait_send()
        for q in (0, 1):
            for k in (1, 2):
                self.z_copy(w, q, k).wait_send()
            for k in (1, 2, 3):
                self.x_copy(w, q, k).wait_send()

            @pl.when(self.inner)
            def _():
                self.z_copy(w, q, 3).wait_send()
                self.z_forward(w, q).wait_send()


def gelu_of(x):
    return 0.5 * x * (1.0 + jnp.tanh(0.7978845608028654 * (x + 0.044715 * (x * x * x))))


def one_less_exp(z):
    series = 1.0 + z * (1.0 / 6.0)
    for order in (5.0, 4.0, 3.0, 2.0):
        series = 1.0 + z * (1.0 / order) * series
    return jnp.where(z > -0.35, -z * series, 1.0 - jnp.exp(z))


def tap_rows(values, taps_ref, cols):
    extent = taps_ref.shape[0]
    summed = taps_ref[extent - 1 : extent, cols] * values
    row = lax.broadcasted_iota(jnp.int32, values.shape, 0)
    for back in range(1, extent):
        moved = jnp.where(row >= back, pltpu.roll(values, back, 0), 0.0)
        summed = summed + taps_ref[extent - 1 - back : extent - back, cols] * moved
    return summed


def dot32(a, b):
    return jnp.dot(a, b, preferred_element_type=jnp.float32)


def layer_kernel(n, *refs):
    sources = refs[:6]
    (stream, reset_map, admit_map, decay_base, taps, spike) = refs[6:12]
    (gate_taps, value_taps, rec_gain, ffn_gain, last_gain, out) = refs[12:18]
    targets = refs[18:24]
    (whole, spike_in, normed, gate_src, decay, inflow, mixed) = refs[24:31]
    (away, landed, kept, share, share_in, middle, middle_in, gate_up, hidden) = refs[31:40]
    (terms, landed_down, down, down_own, down_in, final, sums, sums_in) = refs[40:48]
    gather_sems = refs[48:55]
    (keep_sem, pair_send, pair_recv, near_send, near_recv, far_send, far_recv) = refs[55:]
    tokens, width = stream.shape
    me = lax.axis_index("tp")
    gather = PairGather(n, sources, targets, gather_sems)
    side = gather.y
    bf16, f32 = jnp.bfloat16, jnp.float32
    tile = 256
    strip = 48
    channels = width // 2
    units = hidden.shape[1]
    chunks = 4
    chunk = 2 * tokens // chunks

    def near(i, source, target):
        return gather.copy(source, target, near_send.at[i], near_recv.at[i], {"tp": 1 - me})

    def far(i, source, target):
        return gather.copy(
            source, target, far_send.at[i], far_recv.at[i], {"fs": gather.member(0, 1)}
        )

    def pair(i, source, target):
        return gather.copy(source, target, pair_send.at[i], pair_recv.at[i], {"tp": 1 - me})

    def half(which):
        return pl.ds(pl.multiple_of(which * width, 128), width)

    def strips(lower, upper, body):
        def step(i, carry):
            body(pl.ds(pl.multiple_of(lower + i * strip, 16), strip))
            return carry

        lax.fori_loop(0, (upper - lower) // strip, step, 0)

    def norm_rows(lower, upper, mine, theirs, gain):
        def body(rows):
            a = mine(rows).astype(f32)
            b = theirs(rows).astype(f32)
            total = jnp.sum(a * a, axis=1, keepdims=True) + jnp.sum(b * b, axis=1, keepdims=True)
            inverse = lax.rsqrt(total * (1.0 / (2 * width)) + EPS)
            normed[rows, half(me)] = (a * inverse * gain[:, half(me)]).astype(bf16)
            normed[rows, half(1 - me)] = (b * inverse * gain[:, half(1 - me)]).astype(bf16)

        strips(lower, upper, body)

    first_rows, second_rows = pl.ds(0, tokens), pl.ds(tokens, tokens)
    mine_in = lambda rows: whole[rows, half(me)]
    theirs_in = lambda rows: whole[rows, half(1 - me)]

    arrivals = [(2, 0), (1, 0), (2, 1), (1, 1), (3, 0), (3, 1)]
    served = [0]

    def begin(w):
        gather.z_start(w, 0)
        gather.cross(w)

    def pump(upto):
        while served[0] < upto:
            at = served[0]
            w, step = at // 6, at % 6
            k, q = arrivals[step]
            gather.serve(w, q, k)
            served[0] = at + 1
            if step == 3 and w + 2 < 6:
                begin(w + 2)
            if at == 6:
                for i in (0, 1):
                    for later in (3, 4, 5):
                        gather.y_copy(later, i).start()

    gather.enter()
    own_half = near(0, stream, whole.at[first_rows, half(me)])
    own_half.start()
    for w in range(3):
        gather.y_copy(w, 0).start()
    gather.z_start(0, 0)
    sent_half = far(0, stream, whole.at[second_rows, half(me)])
    sent_half.start()
    sent_spike = far(1, spike, spike_in)
    sent_spike.start()
    for w in range(3):
        gather.y_copy(w, 1).start()
    keep = pltpu.make_async_copy(stream, whole.at[first_rows, half(me)], keep_sem.at[0])
    keep.start()
    for w in range(6):
        for r in (0, 1):
            gather.local(w, r).start()
    gather.cross(0)
    begin(1)
    pump(4)
    keep.wait()
    own_half.wait()
    norm_rows(0, tokens, mine_in, theirs_in, rec_gain)
    pump(6)
    sent_half.wait()
    sent_spike.wait()
    passed = whole.at[second_rows, half(me)]
    pass_on = near(1, passed, passed)
    pass_on.start()
    pump(8)
    pass_on.wait()
    norm_rows(tokens, 2 * tokens, mine_in, theirs_in, rec_gain)
    pump(14)
    gather.ready(0)
    gather.ready(1)

    row_sets = [pl.ds(s * tokens, tokens) for s in (0, 1)]
    base = side * channels

    def wide(start, size):
        return pl.ds(pl.multiple_of(start, 128), size)

    for c in range(channels // tile):
        cols = slice(c * tile, (c + 1) * tile)
        for s in (0, 1):
            rows = row_sets[s]
            rec = dot32(normed[rows, :], targets[0][:, cols]).astype(bf16).astype(f32)
            conv = tap_rows(rec, taps, wide(base + c * tile, tile)).astype(bf16)
            gate_src[rows, cols] = dot32(normed[rows, :], targets[1][:, cols]).astype(bf16)
            spikes = spike if s == 0 else spike_in
            for part in range(tile // 128):
                h = c * (tile // 128) + part
                heads = channels // 128
                lanes = slice(h * 128, (h + 1) * 128)
                block = conv[:, part * 128 : (part + 1) * 128]
                reset = jax.nn.sigmoid(dot32(block, reset_map[side * heads + h]))
                admit = jax.nn.sigmoid(dot32(block, admit_map[side * heads + h]))
                events = jnp.where(
                    side == 0, spikes[:, h : h + 1], spikes[:, heads + h : heads + h + 1]
                )
                log_decay = events - reset * decay_base[:, wide(base + h * 128, 128)]
                decay[rows, lanes] = jnp.exp(log_decay)
                inflow[rows, lanes] = (
                    jnp.sqrt(one_less_exp(2.0 * log_decay)) * admit * block.astype(f32)
                )
            pump(15 + 2 * c + s)

    row = lax.broadcasted_iota(jnp.int32, (8, channels), 0)

    def scan_step(i, carry):
        passed_on = []
        for s in (0, 1):
            rows = pl.ds(pl.multiple_of(s * tokens + i * 16, 16), 16)
            a16, b16 = decay[rows, :], inflow[rows, :]
            state = carry[s]
            found = []
            for part in range(2):
                a, b = a16[part * 8 : part * 8 + 8], b16[part * 8 : part * 8 + 8]
                for back in (1, 2, 4):
                    a_before = jnp.where(row >= back, pltpu.roll(a, back, 0), 1.0)
                    b_before = jnp.where(row >= back, pltpu.roll(b, back, 0), 0.0)
                    b = a * b_before + b
                    a = a * a_before
                states = a * state + b
                state = states[7:8, :]
                found.append(states)
            states = jnp.concatenate(found, axis=0)
            mixed[rows, :] = (states * gelu_of(gate_src[rows, :].astype(f32))).astype(bf16)
            passed_on.append(state)
        return tuple(passed_on)

    still = jnp.zeros((1, channels), f32)
    halfway = tokens // 32
    carry = lax.fori_loop(0, halfway, scan_step, (still, still))
    pump(19)
    lax.fori_loop(halfway, tokens // 16, scan_step, carry)
    gather.ready(2)

    per_half = n // 2
    depth = channels

    def block_of(w, slot, depth):
        return targets[w][pl.ds(pl.multiple_of(slot * depth, 16), depth), :]

    def away_step(j, carry):
        cols = wide(j * tile, tile)
        away[:, cols] = dot32(mixed[...], block_of(2, (1 - me) * per_half + j, depth)).astype(bf16)
        near(2 + j, away.at[:, cols], landed.at[:, cols]).start()
        return carry

    def keep_step(j, carry):
        cols = wide(j * tile, tile)
        kept[:, cols] = dot32(mixed[...], block_of(2, me * per_half + j, depth)).astype(bf16)
        return carry

    lax.fori_loop(0, per_half, away_step, 0)
    lax.fori_loop(0, per_half, keep_step, 0)
    for j in range(per_half):
        cols = slice(j * tile, (j + 1) * tile)
        near(2 + j, away.at[:, cols], landed.at[:, cols]).wait()

    def share_rows(rows):
        share[rows, :] = (kept[rows, :].astype(f32) + landed[rows, :].astype(f32)).astype(bf16)

    def share_copy(i):
        rows = pl.ds((i + chunks // 2) % chunks * chunk, chunk)
        return far(2 + i, share.at[rows, :], share_in.at[pl.ds(i * chunk, chunk), :])

    def middle_copy(i):
        rows = pl.ds(i * chunk, chunk)
        return pair(i, middle.at[rows, :], middle_in.at[rows, :])

    for i in range(chunks):
        lower = (i + chunks // 2) % chunks * chunk
        strips(lower, lower + chunk, share_rows)
        share_copy(i).start()

    def add_branch(rows):
        branch = (share[rows, :].astype(f32) + share_in[rows, :].astype(f32)).astype(bf16)
        middle[rows, :] = (whole[rows, half(me)].astype(f32) + branch.astype(f32)).astype(bf16)

    for i in range(chunks):
        pump((20, 22, 23, 24)[i])
        share_copy(i).wait()
        strips(i * chunk, (i + 1) * chunk, add_branch)
        middle_copy(i).start()
        pump((21, 22, 23, 25)[i])
        middle_copy(i).wait()
        norm_rows(
            i * chunk,
            (i + 1) * chunk,
            lambda rows: middle[rows, :],
            lambda rows: middle_in[rows, :],
            ffn_gain,
        )
    gather.ready(3)

    unit_base = side * units
    tiles = units // tile

    def gate_step(j, carry):
        cols = wide(j * tile, tile)
        gate_up[:, cols] = dot32(normed[...], targets[3][:, cols]).astype(bf16)
        return carry

    for j in range(tiles):
        lax.fori_loop(j, j + 1, gate_step, 0)
        pump(26 + j // 2)
    pump(31)
    gather.ready(4)

    def up_step(j, carry):
        cols = wide(j * tile, tile)
        for s in (0, 1):
            rows = row_sets[s]
            picked = wide(unit_base + j * tile, tile)
            value = dot32(normed[rows, :], targets[4][:, cols]).astype(bf16).astype(f32)
            value = tap_rows(value, value_taps, picked)
            gate = gelu_of(tap_rows(gate_up[rows, cols].astype(f32), gate_taps, picked))
            hidden[rows, cols] = (gate * value).astype(bf16)
        return carry

    for j in range(tiles):
        lax.fori_loop(j, j + 1, up_step, 0)
        pump(min(32 + j, 34))

    low = gather.z // 2
    order = [(0, 0), (0, 1)] + arrivals

    def owned(k):
        return (me == low) if k in (0, 1) else (me == 1 - low)

    def slot_of(i):
        k, q = order[i]
        return gather.member(k, q)

    def down_copy(i):
        cols = wide(slot_of(i) * tile, tile)
        place = wide(lax.rem(slot_of(i), per_half) * tile, tile)
        return near(2 + per_half + i, terms.at[:, cols], landed_down.at[:, place])

    def down_far(i):
        place = wide(lax.rem(slot_of(i), per_half) * tile, tile)
        slot = lax.rem(slot_of(i), per_half)
        return gather.copy(
            down.at[:, place],
            down_in.at[:, place],
            far_send.at[2 + chunks + slot],
            far_recv.at[2 + chunks + slot],
            {"fs": gather.member(0, 1)},
        )

    def fold(i):
        @pl.when(owned(order[i][0]))
        def _():
            down_copy(i).wait_recv()
            cols = wide(slot_of(i) * tile, tile)
            place = wide(lax.rem(slot_of(i), per_half) * tile, tile)

            def far_rows(r, carry):
                rows = pl.ds(pl.multiple_of(r * 128, 16), 128)
                later = pl.ds(pl.multiple_of(tokens + r * 128, 16), 128)
                down[rows, place] = (
                    terms[later, cols].astype(f32) + landed_down[later, place].astype(f32)
                ).astype(bf16)
                return carry

            lax.fori_loop(0, tokens // 128, far_rows, 0)
            down_far(i).start()

            def own_rows(r, carry):
                rows = pl.ds(pl.multiple_of(r * 128, 16), 128)
                down_own[rows, place] = (
                    terms[rows, cols].astype(f32) + landed_down[rows, place].astype(f32)
                ).astype(bf16)
                return carry

            lax.fori_loop(0, tokens // 128, own_rows, 0)

    for i in range(len(order)):
        k, q = order[i]
        if k == 0 and q == 0:
            gather.own_ready(5)
        if k > 0:
            pump(min(30 + i, 36))
            gather.x_arrival(5, q, k).wait_recv()
        cols = wide(slot_of(i) * tile, tile)
        terms[:, cols] = dot32(hidden[...], block_of(5, slot_of(i), units)).astype(bf16)

        @pl.when(jnp.logical_not(owned(k)))
        def _():
            down_copy(i).start()

        if i > 0:
            fold(i - 1)
    fold(len(order) - 1)
    for i in range(len(order)):

        @pl.when(owned(order[i][0]))
        def _():
            down_far(i).wait()

        @pl.when(jnp.logical_not(owned(order[i][0])))
        def _():
            down_copy(i).wait_send()

    def finish(rows):
        branch = (down_own[rows, :].astype(f32) + down_in[rows, :].astype(f32)).astype(bf16)
        total = middle[rows, :].astype(f32) + branch.astype(f32)
        final[rows, :] = total
        square = jnp.sum(total * total, axis=1, keepdims=True)
        sums[rows, :] = jnp.broadcast_to(square, (strip, 128))

    strips(0, tokens, finish)
    summed = pair(chunks, sums, sums_in)
    summed.start()
    summed.wait()

    def scale(rows):
        square = sums[rows, :] + sums_in[rows, :]
        inverse = lax.rsqrt(square * (1.0 / (2 * width)) + EPS)[:, 0:1]
        out[rows, :] = (final[rows, :] * inverse * last_gain[:, half(me)]).astype(bf16)

    strips(0, tokens, scale)
    for w in range(6):
        gather.drain(w)


def fused_layer(n, weights, others):
    tokens, width = others[0].shape
    units = weights[3].shape[1] // 2
    channels = width // 2
    bf16, f32 = jnp.bfloat16, jnp.float32
    vmem = pltpu.VMEM
    dma = pltpu.SemaphoreType.DMA
    halves = []
    for w in weights:
        if w.shape[0] == 2 * width // n:
            halves.append((n * w.shape[0], w.shape[1] // 2))
        else:
            halves.append((n * w.shape[0] // 2, w.shape[1]))
    both = 2 * tokens
    return pl.pallas_call(
        functools.partial(layer_kernel, n),
        out_shape=jax.ShapeDtypeStruct((tokens, width), bf16),
        in_specs=[pl.BlockSpec(memory_space=pl.ANY)] * 6
        + [pl.BlockSpec(memory_space=vmem)] * len(others),
        out_specs=pl.BlockSpec(memory_space=vmem),
        scratch_shapes=[vmem(shape, w.dtype) for shape, w in zip(halves, weights)]
        + [
            vmem((both, 2 * width), bf16),
            vmem(others[5].shape, f32),
            vmem((both, 2 * width), bf16),
            vmem((both, channels), bf16),
            vmem((both, channels), f32),
            vmem((both, channels), f32),
            vmem((both, channels), bf16),
            vmem((both, width), bf16),
            vmem((both, width), bf16),
            vmem((both, width), bf16),
            vmem((both, width), bf16),
            vmem((both, width), bf16),
            vmem((both, width), bf16),
            vmem((both, width), bf16),
            vmem((both, units), bf16),
            vmem((both, units), bf16),
            vmem((both, 2 * width), bf16),
            vmem((both, width), bf16),
            vmem((tokens, width), bf16),
            vmem((tokens, width), bf16),
            vmem((tokens, width), bf16),
            vmem((tokens, width), f32),
            vmem((tokens, 128), f32),
            vmem((tokens, 128), f32),
            dma((6, 2)),
            dma((6, 2)),
            dma((6, 2)),
            dma((6, 2, 4)),
            dma((6, 2, 4)),
            dma((6, 2, 4)),
            dma((6, 2, 4)),
            dma((1,)),
            dma((5,)),
            dma((5,)),
            dma((2 + n // 2 + n,)),
            dma((2 + n // 2 + n,)),
            dma((6 + n // 2,)),
            dma((6 + n // 2,)),
        ],
        compiler_params=pltpu.CompilerParams(
            collective_id=0, has_side_effects=True, vmem_limit_bytes=66_000_000
        ),
    )(*weights, *others)


def shards(
    ringed,
    stream,
    recurrence_input_weight,
    output_gate_weight,
    recurrence_gate_matrix,
    input_gate_matrix,
    channel_decay_rate,
    recurrence_taps,
    spike_log_decay,
    recurrence_output_weight,
    feedforward_gate_upward,
    feedforward_value_upward,
    feedforward_gate_taps,
    feedforward_value_taps,
    feedforward_down_weight,
    recurrence_norm_gain,
    feedforward_norm_gain,
    closing_norm_gain,
):
    tok_rows = stream.shape[0]
    fs_size = lax.axis_size("fs")
    if ringed:
        return fused_layer(
            fs_size,
            (
                recurrence_input_weight,
                output_gate_weight,
                recurrence_output_weight,
                feedforward_gate_upward,
                feedforward_value_upward,
                feedforward_down_weight,
            ),
            (
                stream,
                recurrence_gate_matrix,
                input_gate_matrix,
                (GATE_POWER * jax.nn.softplus(-channel_decay_rate))[None, :],
                recurrence_taps,
                spike_log_decay,
                feedforward_gate_taps,
                feedforward_value_taps,
                recurrence_norm_gain[None, :],
                feedforward_norm_gain[None, :],
                closing_norm_gain[None, :],
            ),
        )
    weights = [
        lax.all_gather(recurrence_input_weight, "fs", axis=0, tiled=True),
        lax.all_gather(output_gate_weight, "fs", axis=0, tiled=True),
        lax.all_gather(recurrence_output_weight, "fs", axis=1, tiled=True),
        lax.all_gather(feedforward_gate_upward, "fs", axis=0, tiled=True),
        lax.all_gather(feedforward_value_upward, "fs", axis=0, tiled=True),
        lax.all_gather(feedforward_down_weight, "fs", axis=1, tiled=True),
    ]
    head_count = recurrence_gate_matrix.shape[0]
    block_size = recurrence_gate_matrix.shape[1]
    whole_rows = lax.all_gather(stream, "tp", axis=1, tiled=True)
    normed = rms_scale(whole_rows, recurrence_norm_gain)
    rec_sum, gate_sum = fold_pair(
        normed,
        (
            weights[0],
            weights[1],
        ),
    )
    rec_in = rec_sum.astype(jnp.bfloat16)
    gate_src = gate_sum.astype(jnp.bfloat16)
    conv_out = causal_mix(rec_in.astype(jnp.float32), recurrence_taps).astype(jnp.bfloat16)
    blocks = conv_out.reshape(tok_rows, head_count, block_size)
    gate_restart = jax.nn.sigmoid(
        jnp.einsum(
            "thi,hij->thj", blocks, recurrence_gate_matrix, preferred_element_type=jnp.float32
        )
    )
    admit_gate = jax.nn.sigmoid(
        jnp.einsum("thi,hij->thj", blocks, input_gate_matrix, preferred_element_type=jnp.float32)
    )
    decay_base = (GATE_POWER * jax.nn.softplus(-channel_decay_rate)).reshape(head_count, block_size)
    decay_logarithm = -gate_restart * decay_base + spike_log_decay[:, :, None]
    decay_rate = jnp.exp(decay_logarithm)
    inflow = jnp.sqrt(-jnp.expm1(2.0 * decay_logarithm)) * admit_gate * blocks.astype(jnp.float32)
    states = lax.associative_scan(chain_step, (decay_rate, inflow), axis=0)[1]
    mixed_out = (
        states.reshape(tok_rows, head_count * block_size)
        * jax.nn.gelu(gate_src.astype(jnp.float32))
    ).astype(jnp.bfloat16)
    mix_terms = project_with(
        mixed_out, weights[2]
    )
    branch = lax.psum_scatter(
        lax.optimization_barrier(mix_terms).astype(jnp.float32).astype(jnp.bfloat16),
        "tp",
        scatter_dimension=1,
        tiled=True,
    )
    middle = (stream.astype(jnp.float32) + branch.astype(jnp.float32)).astype(jnp.bfloat16)
    whole_middle = lax.all_gather(middle, "tp", axis=1, tiled=True)
    normed_ffn = rms_scale(whole_middle, feedforward_norm_gain)
    gate_sum_ffn, value_sum_ffn = fold_pair(
        normed_ffn,
        (
            weights[3],
            weights[4],
        ),
    )
    gate_up = gate_sum_ffn.astype(jnp.bfloat16)
    value_up = value_sum_ffn.astype(jnp.bfloat16)
    gate_conv = causal_mix(gate_up.astype(jnp.float32), feedforward_gate_taps)
    value_conv = causal_mix(value_up.astype(jnp.float32), feedforward_value_taps)
    hidden = (jax.nn.gelu(gate_conv) * value_conv).astype(jnp.bfloat16)
    down_terms = project_with(
        hidden, weights[5]
    )
    branch_ffn = lax.psum_scatter(
        lax.optimization_barrier(down_terms).astype(jnp.float32).astype(jnp.bfloat16),
        "tp",
        scatter_dimension=1,
        tiled=True,
    )
    final_rows = middle.astype(jnp.float32) + branch_ffn.astype(jnp.float32)
    col_count = final_rows.shape[1]
    square_sum = lax.psum(jnp.sum(final_rows * final_rows, axis=1), "tp")
    inverse = lax.rsqrt(square_sum / (col_count * lax.axis_size("tp")) + EPS)
    gain_part = lax.dynamic_slice_in_dim(
        closing_norm_gain, lax.axis_index("tp") * col_count, col_count
    )
    return (final_rows * inverse[:, None] * gain_part[None, :]).astype(jnp.bfloat16)


def solution(mesh):
    in_specs = (
        P(("rep", "fs"), "tp"),
        P("fs", "tp"),
        P("fs", "tp"),
        P("tp", None, None),
        P("tp", None, None),
        P("tp"),
        P(None, "tp"),
        P(("rep", "fs"), "tp"),
        P("tp", "fs"),
        P("fs", "tp"),
        P("fs", "tp"),
        P(None, "tp"),
        P(None, "tp"),
        P("tp", "fs"),
        P(),
        P(),
        P(),
    )
    out_specs = P(("rep", "fs"), "tp")
    ringed = mesh.shape["rep"] == 2 and mesh.shape["tp"] == 2 and mesh.shape["fs"] == 8
    body = functools.partial(shards, ringed)
    return jax.shard_map(body, mesh=mesh, in_specs=in_specs, out_specs=out_specs, check_vma=False)
```

time: 285 us -> 212 us (0.74)
  Pallas kernels: 281 us -> 207 us
    pallas_call x1, Pallas kernels: 281 us -> 207 us  [fused_layer(): pl.pallas_call(functools.partial(layer_kernel, n), out_shape=jax.ShapeDty...]
where the time goes in v1:
time: 212 us; the launch traced here: 211 us
  Pallas kernels  207 us (98%)
  local copies, waits for them, and re-layouts  2.88 us (1%)
    pallas_call x1, Pallas kernels, fused_layer(): pl.pallas_call(functools.partial(layer_kernel, n), out_shape=jax.ShapeDty...  207 us

profile of v1, /device:TPU:0, one launch (start us, length us, event | category | flops | bytes accessed | tf_op | source)
XLA Modules:
  0.0 211.2 jit_solution(10454483554252004210)
XLA Ops:
  0.0 0.0 copy-start
  0.0 1.3 fusion
  1.3 0.0 copy-done
  1.3 0.8 copy.18.refs_11_
  2.1 207.0 %shard_map.163 = bf16[384,1024]{1,0:T(8,128)(2,1)} custom-call(bf16[256,1024]{1,0:T(8,128)(2,1)} %refs_0_.1, bf16[256,1024]{1,0:T(8,128)(2,1)} %refs_1_.1, bf16[1024,256]{1,0:T(8,128)(2,1)} %refs_2_.1, bf16[256,2048]{1,0:T(8,128)(2,1)} %refs_3_.1, bf16[256,2048]{1,0:T(8,128)(2,1)} %refs_4_.1, bf16[2048,256]{1,0:T(8,128)(2,1)} %refs_5_.1, ...), custom_call_target="tpu_custom_call" | custom-call | tf_op jit(solution)/shard_map/pallas_call | solution.py:638
  209.1 2.1 copy.20
Async XLA Ops:
  0.0 1.3 copy-start

commit v2 on v1

--- a/solution.py
+++ b/solution.py
@@ -43,8 +43,9 @@
 
 
 class PairGather:
-    def __init__(self, n, sources, targets, sems):
+    def __init__(self, n, sources, targets, shifts, sems):
         self.n = n
+        self.shifts = shifts
         self.sources = sources
         self.targets = targets
         (self.local_sem, self.y_send, self.y_recv, self.z_send, self.z_recv, self.x_send, self.x_recv) = sems
@@ -52,16 +53,21 @@
         fs = lax.axis_index("fs")
         self.y = lax.rem(fs, 2)
         self.z = fs // 2
-        self.inner = jnp.logical_and(self.z > 0, self.z < n // 2 - 1)
+        levels = n // 2
+        self.middle = self.z * (levels - 1 - self.z) // (levels - 2)
+        self.inner = self.middle == 1
 
     def level(self, k):
+        levels = self.n // 2
+        across = levels - 1 - self.z
+        beyond = lax.rem(self.z + levels // 2, levels)
         if k == 0:
             return self.z
         if k == 1:
             return self.z + 1 - 2 * lax.rem(self.z, 2)
         if k == 2:
-            return lax.rem(self.z + 2, 4)
-        return 3 - self.z
+            return self.middle * across + (1 - self.middle) * beyond
+        return self.middle * beyond + (1 - self.middle) * across
 
     def side(self, q):
         return lax.rem(self.y + q, 2)
@@ -76,14 +82,22 @@
             {"tp": 1 - lax.axis_index("tp")},
             {"fs": self.member(0, 1)},
             {"fs": self.member(1, 0)},
-            {"fs": self.member(2, 0)},
-            {"fs": self.member(3, 0)},
         ]
         for device in devices:
             pl.semaphore_signal(
                 barrier, inc=1, device_id=device, device_id_type=pl.DeviceIdType.MESH
             )
-        pl.semaphore_wait(barrier, len(devices))
+
+        @pl.when(self.inner)
+        def _():
+            pl.semaphore_signal(
+                barrier,
+                inc=1,
+                device_id={"fs": self.member(2, 0)},
+                device_id_type=pl.DeviceIdType.MESH,
+            )
+
+        pl.semaphore_wait(barrier, len(devices) + self.middle)
 
     def depth(self, w):
         return self.targets[w].shape[0] // self.n
@@ -97,7 +111,8 @@
                 pl.ds(pl.multiple_of(r * part, 16), part),
                 pl.ds(pl.multiple_of(half * cols, 128), cols),
             ]
-        return ref.at[pl.ds(pl.multiple_of(half * depth + r * part, 16), part), :]
+        lower = half * (ref.shape[0] // 2) + self.shifts[w] + r * part
+        return ref.at[pl.ds(pl.multiple_of(lower, 16), part), :]
 
     def piece(self, w, shard, r):
         depth = self.depth(w)
@@ -138,36 +153,34 @@
             target, target, self.y_send.at[w, i], self.y_recv.at[w, i], {"fs": self.member(0, 1)}
         )
 
-    def z_copy(self, w, q, k):
-        target = self.piece(w, self.member(0, q), self.x)
-        source = self.source(w, self.y, self.x) if q == 0 else target
+    def hop(self, w, q, k, level):
+        shard = self.member(k, q)
+        target = self.piece(w, shard, self.x)
+        source = self.source(w, self.y, self.x) if k == 0 and q == 0 else target
+        step = level - self.level(k)
+        lane = step + self.n // 2 - 1
         return self.copy(
             source,
             target,
-            self.z_send.at[w, q, k],
-            self.z_recv.at[w, q, k],
-            {"fs": self.member(k, 0)},
+            self.z_send.at[w, q, lane],
+            self.z_recv.at[w, q, lane],
+            {"fs": 2 * level + self.y},
         )
 
     def z_arrival(self, w, q, k):
         target = self.piece(w, self.member(k, q), self.x)
+        lane = self.z - self.level(k) + self.n // 2 - 1
         return self.copy(
             target,
             target,
-            self.z_send.at[w, q, k],
-            self.z_recv.at[w, q, k],
-            {"fs": self.member(k, 0)},
-        )
-
-    def z_forward(self, w, q):
-        target = self.piece(w, self.member(2, q), self.x)
-        return self.copy(
-            target,
-            target,
-            self.z_send.at[w, q, 0],
-            self.z_recv.at[w, q, 3],
+            self.z_send.at[w, q, lane],
+            self.z_recv.at[w, q, lane],
             {"fs": self.member(1, 0)},
         )
+
+    def onward(self, w, q, k):
+        level = self.level(2) if k == 1 else self.level(1)
+        return self.hop(w, q, k, level)
 
     def x_copy(self, w, q, k):
         target = self.piece(w, self.member(k, q), self.x)
@@ -181,27 +194,53 @@
             target, target, self.x_send.at[w, q, k], self.x_recv.at[w, q, k], {"rep": 1 - self.x}
         )
 
-    def z_start(self, w, q):
-        for k in (2, 1):
-            self.z_copy(w, q, k).start()
-
+    def end_start(self, w, q):
+        @pl.when(jnp.logical_not(self.inner))
+        def _():
+            self.hop(w, q, 0, self.level(1)).start()
+
+    def inner_start(self, w, q):
         @pl.when(self.inner)
         def _():
-            self.z_copy(w, q, 3).start()
+            self.hop(w, q, 0, self.level(1)).start()
+            self.hop(w, q, 0, self.level(2)).start()
+
+    def z_start(self, w, q):
+        self.hop(w, q, 0, self.level(1)).start()
+
+        @pl.when(self.inner)
+        def _():
+            self.hop(w, q, 0, self.level(2)).start()
+
+    def crossed(self, w):
+        self.y_arrival(w, 0).wait_recv()
 
     def cross(self, w):
-        self.y_arrival(w, 0).wait_recv()
+        self.crossed(w)
         self.z_start(w, 1)
 
     def serve(self, w, q, k):
         self.z_arrival(w, q, k).wait_recv()
-        if k == 2:
-
-            @pl.when(self.inner)
-            def _():
-                self.z_forward(w, q).start()
+
+        @pl.when(self.inner)
+        def _():
+            self.onward(w, q, k).start()
 
         self.x_copy(w, q, k).start()
+
+    def split_serve(self, at_end, at_inner):
+        @pl.when(self.inner)
+        def _():
+            w, k, q = at_inner
+            self.z_arrival(w, q, k).wait_recv()
+            self.onward(w, q, k).start()
+            self.x_copy(w, q, k).start()
+
+        @pl.when(jnp.logical_not(self.inner))
+        def _():
+            w, k, q = at_end
+            self.z_arrival(w, q, k).wait_recv()
+            self.x_copy(w, q, k).start()
 
     def own_ready(self, w):
         for r in (0, 1):
@@ -218,15 +257,15 @@
         for i in (0, 1):
             self.y_copy(w, i).wait_send()
         for q in (0, 1):
-            for k in (1, 2):
-                self.z_copy(w, q, k).wait_send()
+            self.hop(w, q, 0, self.level(1)).wait_send()
             for k in (1, 2, 3):
                 self.x_copy(w, q, k).wait_send()
 
             @pl.when(self.inner)
             def _():
-                self.z_copy(w, q, 3).wait_send()
-                self.z_forward(w, q).wait_send()
+                self.hop(w, q, 0, self.level(2)).wait_send()
+                for k in (1, 2, 3):
+                    self.onward(w, q, k).wait_send()
 
 
 def gelu_of(x):
@@ -255,18 +294,20 @@
 
 
 def layer_kernel(n, *refs):
-    sources = refs[:6]
-    (stream, reset_map, admit_map, decay_base, taps, spike) = refs[6:12]
+    sources = refs[:6] + refs[5:6]
+    (stream, reset_map, admit_map, decay_rate, taps, spike) = refs[6:12]
     (gate_taps, value_taps, rec_gain, ffn_gain, last_gain, out) = refs[12:18]
-    targets = refs[18:24]
-    (whole, spike_in, normed, gate_src, decay, inflow, mixed) = refs[24:31]
-    (away, landed, kept, share, share_in, middle, middle_in, gate_up, hidden) = refs[31:40]
-    (terms, landed_down, down, down_own, down_in, final, sums, sums_in) = refs[40:48]
-    gather_sems = refs[48:55]
-    (keep_sem, pair_send, pair_recv, near_send, near_recv, far_send, far_recv) = refs[55:]
+    targets = refs[18:25]
+    (whole, spike_in, normed, gate_src, decay, inflow, mixed) = refs[25:32]
+    (away, landed, kept, share, share_in, middle, middle_in, gate_up, hidden) = refs[32:41]
+    (terms, landed_down, down, down_own, down_in, final, sums, sums_in) = refs[41:49]
+    gather_sems = refs[49:56]
+    (keep_sem, pair_send, pair_recv, near_send, near_recv, far_send, far_recv) = refs[56:]
     tokens, width = stream.shape
     me = lax.axis_index("tp")
-    gather = PairGather(n, sources, targets, gather_sems)
+    shifts = [0] * 6 + [targets[5].shape[0] // n]
+    gather = PairGather(n, sources, targets, shifts, gather_sems)
+    last = len(targets) - 1
     side = gather.y
     bf16, f32 = jnp.bfloat16, jnp.float32
     tile = 256
@@ -312,65 +353,90 @@
     mine_in = lambda rows: whole[rows, half(me)]
     theirs_in = lambda rows: whole[rows, half(1 - me)]
 
-    arrivals = [(2, 0), (1, 0), (2, 1), (1, 1), (3, 0), (3, 1)]
+    arrivals = [(k, q) for k in (1, 2, 3) for q in (0, 1)]
+    opening = [(0, 1, 0), (1, 1, 0), (0, 1, 1), (0, 2, 0), (1, 1, 1), (0, 2, 1), (0, 3, 0), (0, 3, 1)]
+    inner_opening = [opening[i] for i in (0, 3, 1, 2, 5, 4, 6, 7)]
+    steady = []
+    for w in range(1, last + 1):
+        steady += [(w, 2, 0), (w, 2, 1)]
+        for q in (0, 1):
+            steady.append((w, 3, q))
+            if w < last:
+                steady.append((w + 1, 1, q))
+    plan, inner_plan = opening + steady, inner_opening + steady
     served = [0]
-
-    def begin(w):
-        gather.z_start(w, 0)
-        gather.cross(w)
 
     def pump(upto):
         while served[0] < upto:
-            at = served[0]
-            w, step = at // 6, at % 6
-            k, q = arrivals[step]
-            gather.serve(w, q, k)
-            served[0] = at + 1
-            if step == 3 and w + 2 < 6:
-                begin(w + 2)
-            if at == 6:
-                for i in (0, 1):
-                    for later in (3, 4, 5):
-                        gather.y_copy(later, i).start()
-
+            w, k, q = plan[served[0]]
+            if plan[served[0]] == inner_plan[served[0]]:
+                gather.serve(w, q, k)
+            else:
+                gather.split_serve(plan[served[0]], inner_plan[served[0]])
+            served[0] += 1
+            if 0 < w < last:
+                if (k, q) == (1, 1):
+                    gather.end_start(w + 1, 0)
+                if (k, q) == (2, 1):
+                    gather.crossed(w + 1)
+                    gather.end_start(w + 1, 1)
+                if k == 3:
+                    gather.inner_start(w + 1, q)
+            if served[0] == 4:
+                gather.y_copy(3, 0).start()
+                sent_spike.start()
+                gather.y_copy(2, 1).start()
+            if served[0] == 9:
+                gather.y_copy(4, 0).start()
+                gather.y_copy(5, 0).start()
+                gather.y_copy(6, 0).start()
+                gather.y_copy(3, 1).start()
+
+    sent_spike = far(1, spike, spike_in)
     gather.enter()
     own_half = near(0, stream, whole.at[first_rows, half(me)])
     own_half.start()
-    for w in range(3):
-        gather.y_copy(w, 0).start()
+    gather.y_copy(0, 0).start()
     gather.z_start(0, 0)
+    gather.y_copy(1, 0).start()
+    gather.y_copy(2, 0).start()
     sent_half = far(0, stream, whole.at[second_rows, half(me)])
     sent_half.start()
-    sent_spike = far(1, spike, spike_in)
-    sent_spike.start()
-    for w in range(3):
-        gather.y_copy(w, 1).start()
+    gather.y_copy(0, 1).start()
+    gather.y_copy(1, 1).start()
     keep = pltpu.make_async_copy(stream, whole.at[first_rows, half(me)], keep_sem.at[0])
     keep.start()
-    for w in range(6):
+    gather.z_start(1, 0)
+    for w in range(last + 1):
         for r in (0, 1):
             gather.local(w, r).start()
     gather.cross(0)
-    begin(1)
-    pump(4)
+    pump(2)
+    gather.cross(1)
+    pump(8)
     keep.wait()
     own_half.wait()
     norm_rows(0, tokens, mine_in, theirs_in, rec_gain)
-    pump(6)
+    pump(10)
     sent_half.wait()
-    sent_spike.wait()
     passed = whole.at[second_rows, half(me)]
     pass_on = near(1, passed, passed)
     pass_on.start()
-    pump(8)
+    pump(11)
     pass_on.wait()
     norm_rows(tokens, 2 * tokens, mine_in, theirs_in, rec_gain)
-    pump(14)
+    pump(16)
     gather.ready(0)
     gather.ready(1)
-
+    sent_spike.wait()
+
+    events_of = [spike[...].T, spike_in[...].T]
     row_sets = [pl.ds(s * tokens, tokens) for s in (0, 1)]
     base = side * channels
+
+    def decay_base(cols):
+        rate = -decay_rate[:, cols]
+        return GATE_POWER * (jnp.maximum(rate, 0.0) + jnp.log1p(jnp.exp(-jnp.abs(rate))))
 
     def wide(start, size):
         return pl.ds(pl.multiple_of(start, 128), size)
@@ -382,7 +448,7 @@
             rec = dot32(normed[rows, :], targets[0][:, cols]).astype(bf16).astype(f32)
             conv = tap_rows(rec, taps, wide(base + c * tile, tile)).astype(bf16)
             gate_src[rows, cols] = dot32(normed[rows, :], targets[1][:, cols]).astype(bf16)
-            spikes = spike if s == 0 else spike_in
+            spikes = events_of[s]
             for part in range(tile // 128):
                 h = c * (tile // 128) + part
                 heads = channels // 128
@@ -393,12 +459,12 @@
                 events = jnp.where(
                     side == 0, spikes[:, h : h + 1], spikes[:, heads + h : heads + h + 1]
                 )
-                log_decay = events - reset * decay_base[:, wide(base + h * 128, 128)]
+                log_decay = events - reset * decay_base(wide(base + h * 128, 128))
                 decay[rows, lanes] = jnp.exp(log_decay)
                 inflow[rows, lanes] = (
                     jnp.sqrt(one_less_exp(2.0 * log_decay)) * admit * block.astype(f32)
                 )
-            pump(15 + 2 * c + s)
+            pump(17 + c * s)
 
     row = lax.broadcasted_iota(jnp.int32, (8, channels), 0)
 
@@ -469,17 +535,19 @@
         lower = (i + chunks // 2) % chunks * chunk
         strips(lower, lower + chunk, share_rows)
         share_copy(i).start()
+    for later in (4, 5, 6):
+        gather.y_copy(later, 1).start()
 
     def add_branch(rows):
         branch = (share[rows, :].astype(f32) + share_in[rows, :].astype(f32)).astype(bf16)
         middle[rows, :] = (whole[rows, half(me)].astype(f32) + branch.astype(f32)).astype(bf16)
 
     for i in range(chunks):
-        pump((20, 22, 23, 24)[i])
+        pump((22, 24, 25, 27)[i])
         share_copy(i).wait()
         strips(i * chunk, (i + 1) * chunk, add_branch)
         middle_copy(i).start()
-        pump((21, 22, 23, 25)[i])
+        pump((23, 25, 26, 27)[i])
         middle_copy(i).wait()
         norm_rows(
             i * chunk,
@@ -500,8 +568,8 @@
 
     for j in range(tiles):
         lax.fori_loop(j, j + 1, gate_step, 0)
-        pump(26 + j // 2)
-    pump(31)
+        pump((28, 28, 29, 29)[j])
+    pump(35)
     gather.ready(4)
 
     def up_step(j, carry):
@@ -517,7 +585,7 @@
 
     for j in range(tiles):
         lax.fori_loop(j, j + 1, up_step, 0)
-        pump(min(32 + j, 34))
+        pump((35, 36, 36, 37)[j])
 
     low = gather.z // 2
     order = [(0, 0), (0, 1)] + arrivals
@@ -529,84 +597,111 @@
         k, q = order[i]
         return gather.member(k, q)
 
-    def down_copy(i):
+    def place_of(i):
+        return wide(lax.rem(slot_of(i), per_half) * tile, tile)
+
+    def down_copy(i, s):
         cols = wide(slot_of(i) * tile, tile)
-        place = wide(lax.rem(slot_of(i), per_half) * tile, tile)
-        return near(2 + per_half + i, terms.at[:, cols], landed_down.at[:, place])
+        rows = row_sets[s]
+        return near(
+            2 + per_half + 2 * i + s, terms.at[rows, cols], landed_down.at[rows, place_of(i)]
+        )
 
     def down_far(i):
-        place = wide(lax.rem(slot_of(i), per_half) * tile, tile)
-        slot = lax.rem(slot_of(i), per_half)
+        place = place_of(i)
+        at = 2 + chunks + lax.rem(slot_of(i), per_half)
         return gather.copy(
             down.at[:, place],
             down_in.at[:, place],
-            far_send.at[2 + chunks + slot],
-            far_recv.at[2 + chunks + slot],
+            far_send.at[at],
+            far_recv.at[at],
             {"fs": gather.member(0, 1)},
         )
+
+    block_rows = 128
+
+    def blocks(body):
+        def step(r, carry):
+            body(pl.multiple_of(r * block_rows, 16))
+            return carry
+
+        lax.fori_loop(0, tokens // block_rows, step, 0)
 
     def fold(i):
         @pl.when(owned(order[i][0]))
         def _():
-            down_copy(i).wait_recv()
-            cols = wide(slot_of(i) * tile, tile)
-            place = wide(lax.rem(slot_of(i), per_half) * tile, tile)
-
-            def far_rows(r, carry):
-                rows = pl.ds(pl.multiple_of(r * 128, 16), 128)
-                later = pl.ds(pl.multiple_of(tokens + r * 128, 16), 128)
-                down[rows, place] = (
-                    terms[later, cols].astype(f32) + landed_down[later, place].astype(f32)
-                ).astype(bf16)
-                return carry
-
-            lax.fori_loop(0, tokens // 128, far_rows, 0)
+            cols, place = wide(slot_of(i) * tile, tile), place_of(i)
+
+            def folded(lower):
+                rows = pl.ds(lower, block_rows)
+                return (terms[rows, cols].astype(f32) + landed_down[rows, place].astype(f32)).astype(
+                    bf16
+                )
+
+            def far_rows(lower):
+                down[pl.ds(lower, block_rows), place] = folded(tokens + lower)
+
+            def own_rows(lower):
+                down_own[pl.ds(lower, block_rows), place] = folded(lower)
+
+            down_copy(i, 1).wait_recv()
+            blocks(far_rows)
             down_far(i).start()
-
-            def own_rows(r, carry):
-                rows = pl.ds(pl.multiple_of(r * 128, 16), 128)
-                down_own[rows, place] = (
-                    terms[rows, cols].astype(f32) + landed_down[rows, place].astype(f32)
-                ).astype(bf16)
-                return carry
-
-            lax.fori_loop(0, tokens // 128, own_rows, 0)
-
+            down_copy(i, 0).wait_recv()
+            blocks(own_rows)
+
+    def finish(i):
+        @pl.when(owned(order[i][0]))
+        def _():
+            place = place_of(i)
+            down_far(i).wait()
+
+            def body(lower):
+                rows = pl.ds(lower, block_rows)
+                branch = down_own[rows, place].astype(f32) + down_in[rows, place].astype(f32)
+                total = middle[rows, place].astype(f32) + branch.astype(bf16).astype(f32)
+                final[rows, place] = total
+                square = jnp.sum(total * total, axis=1, keepdims=True)
+                before = 0.0 if i in (0, per_half) else sums[rows, :]
+                sums[rows, :] = before + jnp.broadcast_to(square, (block_rows, 128))
+
+            blocks(body)
+
+    cut = units // 2
     for i in range(len(order)):
         k, q = order[i]
-        if k == 0 and q == 0:
+        if i == 0:
             gather.own_ready(5)
+            gather.own_ready(6)
+        pump((37, 38, 39, 41, 42, 42, 42, 42)[i])
         if k > 0:
-            pump(min(30 + i, 36))
             gather.x_arrival(5, q, k).wait_recv()
+            gather.x_arrival(6, q, k).wait_recv()
         cols = wide(slot_of(i) * tile, tile)
-        terms[:, cols] = dot32(hidden[...], block_of(5, slot_of(i), units)).astype(bf16)
-
-        @pl.when(jnp.logical_not(owned(k)))
-        def _():
-            down_copy(i).start()
-
-        if i > 0:
+        for s in (1, 0):
+            rows = row_sets[s]
+            first_cut = dot32(hidden[rows, :cut], block_of(5, slot_of(i), cut))
+            second_cut = dot32(hidden[rows, cut:], block_of(6, slot_of(i), cut))
+            terms[rows, cols] = (first_cut + second_cut).astype(bf16)
+
+            @pl.when(jnp.logical_not(owned(k)))
+            def _():
+                down_copy(i, s).start()
+
+            if s == 1 and i > 5:
+                fold(i - 1)
+        if 0 < i < 6:
             fold(i - 1)
     fold(len(order) - 1)
     for i in range(len(order)):
-
-        @pl.when(owned(order[i][0]))
-        def _():
-            down_far(i).wait()
+        finish(i)
+    for i in range(len(order)):
 
         @pl.when(jnp.logical_not(owned(order[i][0])))
         def _():
-            down_copy(i).wait_send()
-
-    def finish(rows):
-        branch = (down_own[rows, :].astype(f32) + down_in[rows, :].astype(f32)).astype(bf16)
-        total = middle[rows, :].astype(f32) + branch.astype(f32)
-        final[rows, :] = total
-        square = jnp.sum(total * total, axis=1, keepdims=True)
-        sums[rows, :] = jnp.broadcast_to(square, (strip, 128))
-
-    strips(0, tokens, finish)
+            for s in (0, 1):
+                down_copy(i, s).wait_send()
+
     summed = pair(chunks, sums, sums_in)
     summed.start()
     summed.wait()
@@ -617,7 +712,7 @@
         out[rows, :] = (final[rows, :] * inverse * last_gain[:, half(me)]).astype(bf16)
 
     strips(0, tokens, scale)
-    for w in range(6):
+    for w in range(last + 1):
         gather.drain(w)
 
 
@@ -634,6 +729,8 @@
             halves.append((n * w.shape[0], w.shape[1] // 2))
         else:
             halves.append((n * w.shape[0] // 2, w.shape[1]))
+    halves[-1:] = [(halves[-1][0] // 2, halves[-1][1])] * 2
+    parts = len(halves)
     both = 2 * tokens
     return pl.pallas_call(
         functools.partial(layer_kernel, n),
@@ -641,7 +738,7 @@
         in_specs=[pl.BlockSpec(memory_space=pl.ANY)] * 6
         + [pl.BlockSpec(memory_space=vmem)] * len(others),
         out_specs=pl.BlockSpec(memory_space=vmem),
-        scratch_shapes=[vmem(shape, w.dtype) for shape, w in zip(halves, weights)]
+        scratch_shapes=[vmem(shape, bf16) for shape in halves]
         + [
             vmem((both, 2 * width), bf16),
             vmem(others[5].shape, f32),
@@ -667,18 +764,18 @@
             vmem((tokens, width), f32),
             vmem((tokens, 128), f32),
             vmem((tokens, 128), f32),
-            dma((6, 2)),
-            dma((6, 2)),
-            dma((6, 2)),
-            dma((6, 2, 4)),
-            dma((6, 2, 4)),
-            dma((6, 2, 4)),
-            dma((6, 2, 4)),
+            dma((parts, 2)),
+            dma((parts, 2)),
+            dma((parts, 2)),
+            dma((parts, 2, n - 1)),
+            dma((parts, 2, n - 1)),
+            dma((parts, 2, 4)),
+            dma((parts, 2, 4)),
             dma((1,)),
             dma((5,)),
             dma((5,)),
-            dma((2 + n // 2 + n,)),
-            dma((2 + n // 2 + n,)),
+            dma((2 + n // 2 + 2 * n,)),
+            dma((2 + n // 2 + 2 * n,)),
             dma((6 + n // 2,)),
             dma((6 + n // 2,)),
         ],
@@ -725,9 +822,9 @@
                 stream,
                 recurrence_gate_matrix,
                 input_gate_matrix,
-                (GATE_POWER * jax.nn.softplus(-channel_decay_rate))[None, :],
+                channel_decay_rate[None, :],
                 recurrence_taps,
-                spike_log_decay,
+                spike_log_decay.T,
                 feedforward_gate_taps,
                 feedforward_value_taps,
                 recurrence_norm_gain[None, :],

time: 212 us -> 189 us (0.89)
  Pallas kernels: 207 us -> 187 us
    pallas_call x1, Pallas kernels: 207 us -> 187 us  [fused_layer(): pl.pallas_call(functools.partial(layer_kernel, n), out_shape=jax.ShapeDty...]
where the time goes in v2:
time: 189 us
  Pallas kernels  187 us (99%)
  local copies, waits for them, and re-layouts  2.06 us (1%)
    pallas_call x1, Pallas kernels, fused_layer(): pl.pallas_call(functools.partial(layer_kernel, n), out_shape=jax.ShapeDty...  187 us

profile of v2, /device:TPU:0, one launch (start us, length us, event | category | flops | bytes accessed | tf_op | source)
XLA Modules:
  0.0 188.8 jit_solution(4111958575199098378)
XLA Ops:
  0.0 186.7 %shard_map.163 = bf16[384,1024]{1,0:T(8,128)(2,1)} custom-call(bf16[256,1024]{1,0:T(8,128)(2,1)} %refs_0_.1, bf16[256,1024]{1,0:T(8,128)(2,1)} %refs_1_.1, bf16[1024,256]{1,0:T(8,128)(2,1)} %refs_2_.1, bf16[256,2048]{1,0:T(8,128)(2,1)} %refs_3_.1, bf16[256,2048]{1,0:T(8,128)(2,1)} %refs_4_.1, bf16[2048,256]{1,0:T(8,128)(2,1)} %refs_5_.1, ...), custom_call_target="tpu_custom_call" | custom-call | tf_op jit(solution)/shard_map/pallas_call | solution.py:735
  186.7 2.1 %copy.19 = bf16[384,1024]{1,0:T(8,128)(2,1)} copy(bf16[384,1024]{1,0:T(8,128)(2,1)} %shard_map.163) | data formatting | bytes 1572864

commit v3 on v2

--- a/solution.py
+++ b/solution.py
@@ -107,9 +107,10 @@
         part = depth // 2
         cols = self.targets[w].shape[1]
         if ref.shape[0] == depth:
+            lower = half * (ref.shape[1] // 2) + self.shifts[w]
             return ref.at[
                 pl.ds(pl.multiple_of(r * part, 16), part),
-                pl.ds(pl.multiple_of(half * cols, 128), cols),
+                pl.ds(pl.multiple_of(lower, 128), cols),
             ]
         lower = half * (ref.shape[0] // 2) + self.shifts[w] + r * part
         return ref.at[pl.ds(pl.multiple_of(lower, 16), part), :]
@@ -212,6 +213,14 @@
         def _():
             self.hop(w, q, 0, self.level(2)).start()
 
+    def edge_start(self, w, q):
+        self.hop(w, q, 0, self.level(1)).start()
+
+    def core_start(self, w, q):
+        @pl.when(self.inner)
+        def _():
+            self.hop(w, q, 0, self.level(2)).start()
+
     def crossed(self, w):
         self.y_arrival(w, 0).wait_recv()
 
@@ -294,18 +303,19 @@
 
 
 def layer_kernel(n, *refs):
-    sources = refs[:6] + refs[5:6]
+    sources = [refs[i] for i in (0, 1, 2, 3, 3, 4, 4, 5, 5)]
     (stream, reset_map, admit_map, decay_rate, taps, spike) = refs[6:12]
     (gate_taps, value_taps, rec_gain, ffn_gain, last_gain, out) = refs[12:18]
-    targets = refs[18:25]
-    (whole, spike_in, normed, gate_src, decay, inflow, mixed) = refs[25:32]
-    (away, landed, kept, share, share_in, middle, middle_in, gate_up, hidden) = refs[32:41]
-    (terms, landed_down, down, down_own, down_in, final, sums, sums_in) = refs[41:49]
-    gather_sems = refs[49:56]
-    (keep_sem, pair_send, pair_recv, near_send, near_recv, far_send, far_recv) = refs[56:]
+    targets = refs[18:27]
+    (whole, spike_in, normed, gate_src, decay, inflow, mixed) = refs[27:34]
+    (away, landed, kept, share, share_in, middle, middle_in, gate_up, hidden) = refs[34:43]
+    (terms, landed_down, down, down_own, down_in, final, sums, sums_in) = refs[43:51]
+    gather_sems = refs[51:58]
+    (keep_sem, pair_send, pair_recv, near_send, near_recv, far_send, far_recv) = refs[58:]
     tokens, width = stream.shape
     me = lax.axis_index("tp")
-    shifts = [0] * 6 + [targets[5].shape[0] // n]
+    wide_cut, deep_cut = targets[3].shape[1], targets[7].shape[0] // n
+    shifts = [0, 0, 0, 0, wide_cut, 0, wide_cut, 0, deep_cut]
     gather = PairGather(n, sources, targets, shifts, gather_sems)
     last = len(targets) - 1
     side = gather.y
@@ -355,7 +365,7 @@
 
     arrivals = [(k, q) for k in (1, 2, 3) for q in (0, 1)]
     opening = [(0, 1, 0), (1, 1, 0), (0, 1, 1), (0, 2, 0), (1, 1, 1), (0, 2, 1), (0, 3, 0), (0, 3, 1)]
-    inner_opening = [opening[i] for i in (0, 3, 1, 2, 5, 4, 6, 7)]
+    inner_opening = [opening[i] for i in (0, 3, 2, 5, 1, 4, 6, 7)]
     steady = []
     for w in range(1, last + 1):
         steady += [(w, 2, 0), (w, 2, 1)]
@@ -386,11 +396,12 @@
                 gather.y_copy(3, 0).start()
                 sent_spike.start()
                 gather.y_copy(2, 1).start()
+                gather.y_copy(4, 0).start()
             if served[0] == 9:
-                gather.y_copy(4, 0).start()
-                gather.y_copy(5, 0).start()
-                gather.y_copy(6, 0).start()
-                gather.y_copy(3, 1).start()
+                for later in (5, 6, 7, 8):
+                    gather.y_copy(later, 0).start()
+                for later in (3, 4):
+                    gather.y_copy(later, 1).start()
 
     sent_spike = far(1, spike, spike_in)
     gather.enter()
@@ -406,12 +417,13 @@
     gather.y_copy(1, 1).start()
     keep = pltpu.make_async_copy(stream, whole.at[first_rows, half(me)], keep_sem.at[0])
     keep.start()
-    gather.z_start(1, 0)
+    gather.edge_start(1, 0)
     for w in range(last + 1):
         for r in (0, 1):
             gather.local(w, r).start()
     gather.cross(0)
     pump(2)
+    gather.core_start(1, 0)
     gather.cross(1)
     pump(8)
     keep.wait()
@@ -464,7 +476,7 @@
                 inflow[rows, lanes] = (
                     jnp.sqrt(one_less_exp(2.0 * log_decay)) * admit * block.astype(f32)
                 )
-            pump(17 + c * s)
+            pump(17 + c)
 
     row = lax.broadcasted_iota(jnp.int32, (8, channels), 0)
 
@@ -495,6 +507,7 @@
     carry = lax.fori_loop(0, halfway, scan_step, (still, still))
     pump(19)
     lax.fori_loop(halfway, tokens // 16, scan_step, carry)
+    pump(20)
     gather.ready(2)
 
     per_half = n // 2
@@ -515,7 +528,9 @@
         return carry
 
     lax.fori_loop(0, per_half, away_step, 0)
+    pump(21)
     lax.fori_loop(0, per_half, keep_step, 0)
+    pump(22)
     for j in range(per_half):
         cols = slice(j * tile, (j + 1) * tile)
         near(2 + j, away.at[:, cols], landed.at[:, cols]).wait()
@@ -535,7 +550,7 @@
         lower = (i + chunks // 2) % chunks * chunk
         strips(lower, lower + chunk, share_rows)
         share_copy(i).start()
-    for later in (4, 5, 6):
+    for later in (5, 6, 7, 8):
         gather.y_copy(later, 1).start()
 
     def add_branch(rows):
@@ -543,11 +558,11 @@
         middle[rows, :] = (whole[rows, half(me)].astype(f32) + branch.astype(f32)).astype(bf16)
 
     for i in range(chunks):
-        pump((22, 24, 25, 27)[i])
+        pump((26, 29, 32, 35)[i])
         share_copy(i).wait()
         strips(i * chunk, (i + 1) * chunk, add_branch)
         middle_copy(i).start()
-        pump((23, 25, 26, 27)[i])
+        pump((27, 30, 33, 36)[i])
         middle_copy(i).wait()
         norm_rows(
             i * chunk,
@@ -557,35 +572,39 @@
             ffn_gain,
         )
     gather.ready(3)
+    gather.ready(4)
 
     unit_base = side * units
     tiles = units // tile
-
-    def gate_step(j, carry):
-        cols = wide(j * tile, tile)
-        gate_up[:, cols] = dot32(normed[...], targets[3][:, cols]).astype(bf16)
-        return carry
-
-    for j in range(tiles):
-        lax.fori_loop(j, j + 1, gate_step, 0)
-        pump((28, 28, 29, 29)[j])
-    pump(35)
-    gather.ready(4)
-
-    def up_step(j, carry):
-        cols = wide(j * tile, tile)
+    per_cut = wide_cut // tile
+
+    def gate_step(j):
+        inside = slice(j % per_cut * tile, (j % per_cut + 1) * tile)
+        block = targets[3 + j // per_cut][:, inside]
+        gate_up[:, j * tile : (j + 1) * tile] = dot32(normed[...], block).astype(bf16)
+
+    def up_step(j):
+        cols = slice(j * tile, (j + 1) * tile)
+        inside = slice(j % per_cut * tile, (j % per_cut + 1) * tile)
+        picked = wide(unit_base + j * tile, tile)
         for s in (0, 1):
             rows = row_sets[s]
-            picked = wide(unit_base + j * tile, tile)
-            value = dot32(normed[rows, :], targets[4][:, cols]).astype(bf16).astype(f32)
+            block = targets[5 + j // per_cut][:, inside]
+            value = dot32(normed[rows, :], block).astype(bf16).astype(f32)
             value = tap_rows(value, value_taps, picked)
             gate = gelu_of(tap_rows(gate_up[rows, cols].astype(f32), gate_taps, picked))
             hidden[rows, cols] = (gate * value).astype(bf16)
-        return carry
 
     for j in range(tiles):
-        lax.fori_loop(j, j + 1, up_step, 0)
-        pump((35, 36, 36, 37)[j])
+        gate_step(j)
+        pump((37, 38, 38, 39)[j])
+    gather.ready(5)
+    for j in range(tiles):
+        if j == per_cut:
+            pump(45)
+            gather.ready(6)
+        up_step(j)
+        pump((40, 41, 46, 47)[j])
 
     low = gather.z // 2
     order = [(0, 0), (0, 1)] + arrivals
@@ -627,7 +646,7 @@
 
         lax.fori_loop(0, tokens // block_rows, step, 0)
 
-    def fold(i):
+    def fold(i, s):
         @pl.when(owned(order[i][0]))
         def _():
             cols, place = wide(slot_of(i) * tile, tile), place_of(i)
@@ -644,11 +663,13 @@
             def own_rows(lower):
                 down_own[pl.ds(lower, block_rows), place] = folded(lower)
 
-            down_copy(i, 1).wait_recv()
-            blocks(far_rows)
-            down_far(i).start()
-            down_copy(i, 0).wait_recv()
-            blocks(own_rows)
+            if s == 1:
+                down_copy(i, 1).wait_recv()
+                blocks(far_rows)
+                down_far(i).start()
+            else:
+                down_copy(i, 0).wait_recv()
+                blocks(own_rows)
 
     def finish(i):
         @pl.when(owned(order[i][0]))
@@ -660,7 +681,7 @@
                 rows = pl.ds(lower, block_rows)
                 branch = down_own[rows, place].astype(f32) + down_in[rows, place].astype(f32)
                 total = middle[rows, place].astype(f32) + branch.astype(bf16).astype(f32)
-                final[rows, place] = total
+                final[rows, place] = total * last_gain[:, wide(me * width + place.start, tile)]
                 square = jnp.sum(total * total, axis=1, keepdims=True)
                 before = 0.0 if i in (0, per_half) else sums[rows, :]
                 sums[rows, :] = before + jnp.broadcast_to(square, (block_rows, 128))
@@ -671,28 +692,27 @@
     for i in range(len(order)):
         k, q = order[i]
         if i == 0:
-            gather.own_ready(5)
-            gather.own_ready(6)
-        pump((37, 38, 39, 41, 42, 42, 42, 42)[i])
+            gather.own_ready(7)
+            gather.own_ready(8)
+        pump((48, 49, 50, 52, 53, 54, 54, 54)[i])
         if k > 0:
-            gather.x_arrival(5, q, k).wait_recv()
-            gather.x_arrival(6, q, k).wait_recv()
+            gather.x_arrival(7, q, k).wait_recv()
+            gather.x_arrival(8, q, k).wait_recv()
         cols = wide(slot_of(i) * tile, tile)
         for s in (1, 0):
             rows = row_sets[s]
-            first_cut = dot32(hidden[rows, :cut], block_of(5, slot_of(i), cut))
-            second_cut = dot32(hidden[rows, cut:], block_of(6, slot_of(i), cut))
+            first_cut = dot32(hidden[rows, :cut], block_of(7, slot_of(i), cut))
+            second_cut = dot32(hidden[rows, cut:], block_of(8, slot_of(i), cut))
             terms[rows, cols] = (first_cut + second_cut).astype(bf16)
 
             @pl.when(jnp.logical_not(owned(k)))
             def _():
                 down_copy(i, s).start()
 
-            if s == 1 and i > 5:
-                fold(i - 1)
-        if 0 < i < 6:
-            fold(i - 1)
-    fold(len(order) - 1)
+            if i > 0:
+                fold(i - 1, s)
+    for s in (1, 0):
+        fold(len(order) - 1, s)
     for i in range(len(order)):
         finish(i)
     for i in range(len(order)):
@@ -706,12 +726,13 @@
     summed.start()
     summed.wait()
 
-    def scale(rows):
+    def scale(lower):
+        rows = pl.ds(lower, block_rows)
         square = sums[rows, :] + sums_in[rows, :]
         inverse = lax.rsqrt(square * (1.0 / (2 * width)) + EPS)[:, 0:1]
-        out[rows, :] = (final[rows, :] * inverse * last_gain[:, half(me)]).astype(bf16)
-
-    strips(0, tokens, scale)
+        out[rows, :] = (final[rows, :] * inverse).astype(bf16)
+
+    blocks(scale)
     for w in range(last + 1):
         gather.drain(w)
 
@@ -729,7 +750,8 @@
             halves.append((n * w.shape[0], w.shape[1] // 2))
         else:
             halves.append((n * w.shape[0] // 2, w.shape[1]))
-    halves[-1:] = [(halves[-1][0] // 2, halves[-1][1])] * 2
+    split = [(rows, cols // 2) for rows, cols in halves[3:5] for _ in (0, 1)]
+    halves = halves[:3] + split + [(halves[5][0] // 2, halves[5][1])] * 2
     parts = len(halves)
     both = 2 * tokens
     return pl.pallas_call(

time: 189 us -> 185 us (0.979)
  Pallas kernels: 187 us -> 182 us
    pallas_call x1, Pallas kernels: 187 us -> 182 us  [fused_layer(): pl.pallas_call(functools.partial(layer_kernel, n), out_shape=jax.ShapeDty...]
where the time goes in v3:
time: 185 us; the launch traced here: 184 us
  Pallas kernels  182 us (98%)
  local copies, waits for them, and re-layouts  2.06 us (1%)
    pallas_call x1, Pallas kernels, fused_layer(): pl.pallas_call(functools.partial(layer_kernel, n), out_shape=jax.ShapeDty...  182 us

profile of v3, /device:TPU:0, one launch (start us, length us, event | category | flops | bytes accessed | tf_op | source)
XLA Modules:
  0.0 184.4 jit_solution(3302980463456033203)
XLA Ops:
  0.0 182.4 %shard_map.163 = bf16[384,1024]{1,0:T(8,128)(2,1)} custom-call(bf16[256,1024]{1,0:T(8,128)(2,1)} %refs_0_.1, bf16[256,1024]{1,0:T(8,128)(2,1)} %refs_1_.1, bf16[1024,256]{1,0:T(8,128)(2,1)} %refs_2_.1, bf16[256,2048]{1,0:T(8,128)(2,1)} %refs_3_.1, bf16[256,2048]{1,0:T(8,128)(2,1)} %refs_4_.1, bf16[2048,256]{1,0:T(8,128)(2,1)} %refs_5_.1, ...), custom_call_target="tpu_custom_call" | custom-call | tf_op jit(solution)/shard_map/pallas_call | solution.py:757
  182.4 2.1 %copy.19 = bf16[384,1024]{1,0:T(8,128)(2,1)} copy(bf16[384,1024]{1,0:T(8,128)(2,1)} %shard_map.163) | data formatting | bytes 1572864

commit v4 on v3

--- a/solution.py
+++ b/solution.py
@@ -112,8 +112,8 @@
                 pl.ds(pl.multiple_of(r * part, 16), part),
                 pl.ds(pl.multiple_of(lower, 128), cols),
             ]
-        lower = half * (ref.shape[0] // 2) + self.shifts[w] + r * part
-        return ref.at[pl.ds(pl.multiple_of(lower, 16), part), :]
+        lower = half * depth + r * part
+        return ref.at[pl.ds(pl.multiple_of(lower, 16), part), pl.ds(self.shifts[w], cols)]
 
     def piece(self, w, shard, r):
         depth = self.depth(w)
@@ -130,13 +130,14 @@
             device_id_type=pl.DeviceIdType.MESH,
         )
 
-    def local(self, w, r):
-        return pltpu.make_async_copy(
-            self.source(w, self.y, r), self.piece(w, self.member(0, 0), r), self.local_sem.at[w, r]
-        )
-
     def half_of(self, i):
         return self.x if i == 0 else 1 - self.x
+
+    def local(self, w, i):
+        r = self.half_of(i)
+        return pltpu.make_async_copy(
+            self.source(w, self.y, r), self.piece(w, self.member(0, 0), r), self.local_sem.at[w, i]
+        )
 
     def y_copy(self, w, i):
         r = self.half_of(i)
@@ -157,7 +158,7 @@
     def hop(self, w, q, k, level):
         shard = self.member(k, q)
         target = self.piece(w, shard, self.x)
-        source = self.source(w, self.y, self.x) if k == 0 and q == 0 else target
+        source = self.source(w, self.y, self.x) if k == 0 and q == 0 and w > 0 else target
         step = level - self.level(k)
         lane = step + self.n // 2 - 1
         return self.copy(
@@ -252,8 +253,9 @@
             self.x_copy(w, q, k).start()
 
     def own_ready(self, w):
-        for r in (0, 1):
-            self.local(w, r).wait()
+        if w > 0:
+            self.local(w, 0).wait()
+        self.local(w, 1).wait()
         self.y_arrival(w, 1).wait_recv()
 
     def ready(self, w):
@@ -314,8 +316,8 @@
     (keep_sem, pair_send, pair_recv, near_send, near_recv, far_send, far_recv) = refs[58:]
     tokens, width = stream.shape
     me = lax.axis_index("tp")
-    wide_cut, deep_cut = targets[3].shape[1], targets[7].shape[0] // n
-    shifts = [0, 0, 0, 0, wide_cut, 0, wide_cut, 0, deep_cut]
+    wide_cut, down_cut = targets[3].shape[1], targets[7].shape[1]
+    shifts = [0, 0, 0, 0, wide_cut, 0, wide_cut, 0, down_cut]
     gather = PairGather(n, sources, targets, shifts, gather_sems)
     last = len(targets) - 1
     side = gather.y
@@ -404,13 +406,15 @@
                     gather.y_copy(later, 1).start()
 
     sent_spike = far(1, spike, spike_in)
+    gather.local(0, 0).start()
     gather.enter()
+    gather.local(0, 0).wait()
+    gather.z_start(0, 0)
+    gather.y_copy(0, 0).start()
+    gather.y_copy(1, 0).start()
+    gather.y_copy(2, 0).start()
     own_half = near(0, stream, whole.at[first_rows, half(me)])
     own_half.start()
-    gather.y_copy(0, 0).start()
-    gather.z_start(0, 0)
-    gather.y_copy(1, 0).start()
-    gather.y_copy(2, 0).start()
     sent_half = far(0, stream, whole.at[second_rows, half(me)])
     sent_half.start()
     gather.y_copy(0, 1).start()
@@ -418,9 +422,10 @@
     keep = pltpu.make_async_copy(stream, whole.at[first_rows, half(me)], keep_sem.at[0])
     keep.start()
     gather.edge_start(1, 0)
-    for w in range(last + 1):
-        for r in (0, 1):
-            gather.local(w, r).start()
+    gather.local(0, 1).start()
+    for w in range(1, last + 1):
+        for i in (0, 1):
+            gather.local(w, i).start()
     gather.cross(0)
     pump(2)
     gather.core_start(1, 0)
@@ -607,20 +612,22 @@
         pump((40, 41, 46, 47)[j])
 
     low = gather.z // 2
-    order = [(0, 0), (0, 1)] + arrivals
+    order = [(cut, k, q) for cut in (0, 1) for k, q in [(0, 0), (0, 1)] + arrivals]
 
     def owned(k):
         return (me == low) if k in (0, 1) else (me == 1 - low)
 
     def slot_of(i):
-        k, q = order[i]
-        return gather.member(k, q)
+        return gather.member(order[i][1], order[i][2])
+
+    def cols_of(i):
+        return wide(slot_of(i) * tile + order[i][0] * down_cut, down_cut)
 
     def place_of(i):
-        return wide(lax.rem(slot_of(i), per_half) * tile, tile)
+        return wide(lax.rem(slot_of(i), per_half) * tile + order[i][0] * down_cut, down_cut)
 
     def down_copy(i, s):
-        cols = wide(slot_of(i) * tile, tile)
+        cols = cols_of(i)
         rows = row_sets[s]
         return near(
             2 + per_half + 2 * i + s, terms.at[rows, cols], landed_down.at[rows, place_of(i)]
@@ -628,7 +635,7 @@
 
     def down_far(i):
         place = place_of(i)
-        at = 2 + chunks + lax.rem(slot_of(i), per_half)
+        at = 2 + chunks + 2 * lax.rem(slot_of(i), per_half) + order[i][0]
         return gather.copy(
             down.at[:, place],
             down_in.at[:, place],
@@ -647,9 +654,9 @@
         lax.fori_loop(0, tokens // block_rows, step, 0)
 
     def fold(i, s):
-        @pl.when(owned(order[i][0]))
-        def _():
-            cols, place = wide(slot_of(i) * tile, tile), place_of(i)
+        @pl.when(owned(order[i][1]))
+        def _():
+            cols, place = cols_of(i), place_of(i)
 
             def folded(lower):
                 rows = pl.ds(lower, block_rows)
@@ -672,7 +679,7 @@
                 blocks(own_rows)
 
     def finish(i):
-        @pl.when(owned(order[i][0]))
+        @pl.when(owned(order[i][1]))
         def _():
             place = place_of(i)
             down_far(i).wait()
@@ -681,29 +688,26 @@
                 rows = pl.ds(lower, block_rows)
                 branch = down_own[rows, place].astype(f32) + down_in[rows, place].astype(f32)
                 total = middle[rows, place].astype(f32) + branch.astype(bf16).astype(f32)
-                final[rows, place] = total * last_gain[:, wide(me * width + place.start, tile)]
+                final[rows, place] = total * last_gain[:, wide(me * width + place.start, down_cut)]
                 square = jnp.sum(total * total, axis=1, keepdims=True)
                 before = 0.0 if i in (0, per_half) else sums[rows, :]
                 sums[rows, :] = before + jnp.broadcast_to(square, (block_rows, 128))
 
             blocks(body)
 
-    cut = units // 2
     for i in range(len(order)):
-        k, q = order[i]
+        cut, k, q = order[i]
         if i == 0:
             gather.own_ready(7)
             gather.own_ready(8)
-        pump((48, 49, 50, 52, 53, 54, 54, 54)[i])
+        pump((47, 47, 48, 48, 49, 49, 50, 51, 51, 52, 52, 53, 53, 54, 54, 54)[i])
         if k > 0:
-            gather.x_arrival(7, q, k).wait_recv()
-            gather.x_arrival(8, q, k).wait_recv()
-        cols = wide(slot_of(i) * tile, tile)
+            gather.x_arrival(7 + cut, q, k).wait_recv()
+        cols = cols_of(i)
         for s in (1, 0):
             rows = row_sets[s]
-            first_cut = dot32(hidden[rows, :cut], block_of(7, slot_of(i), cut))
-            second_cut = dot32(hidden[rows, cut:], block_of(8, slot_of(i), cut))
-            terms[rows, cols] = (first_cut + second_cut).astype(bf16)
+            block = block_of(7 + cut, slot_of(i), units)
+            terms[rows, cols] = dot32(hidden[rows, :], block).astype(bf16)
 
             @pl.when(jnp.logical_not(owned(k)))
             def _():
@@ -717,7 +721,7 @@
         finish(i)
     for i in range(len(order)):
 
-        @pl.when(jnp.logical_not(owned(order[i][0])))
+        @pl.when(jnp.logical_not(owned(order[i][1])))
         def _():
             for s in (0, 1):
                 down_copy(i, s).wait_send()
@@ -751,7 +755,7 @@
         else:
             halves.append((n * w.shape[0] // 2, w.shape[1]))
     split = [(rows, cols // 2) for rows, cols in halves[3:5] for _ in (0, 1)]
-    halves = halves[:3] + split + [(halves[5][0] // 2, halves[5][1])] * 2
+    halves = halves[:3] + split + [(halves[5][0], halves[5][1] // 2)] * 2
     parts = len(halves)
     both = 2 * tokens
     return pl.pallas_call(
@@ -796,10 +800,10 @@
             dma((1,)),
             dma((5,)),
             dma((5,)),
-            dma((2 + n // 2 + 2 * n,)),
-            dma((2 + n // 2 + 2 * n,)),
-            dma((6 + n // 2,)),
-            dma((6 + n // 2,)),
+            dma((2 + n // 2 + 4 * n,)),
+            dma((2 + n // 2 + 4 * n,)),
+            dma((6 + n,)),
+            dma((6 + n,)),
         ],
         compiler_params=pltpu.CompilerParams(
             collective_id=0, has_side_effects=True, vmem_limit_bytes=66_000_000

time: 185 us -> 182 us (0.984)
  Pallas kernels: 182 us -> 180 us
    pallas_call x1, Pallas kernels: 182 us -> 180 us  [fused_layer(): pl.pallas_call(functools.partial(layer_kernel, n), out_shape=jax.ShapeDty...]
where the time goes in v4:
time: 182 us
  Pallas kernels  180 us (99%)
  local copies, waits for them, and re-layouts  2.06 us (1%)
    pallas_call x1, Pallas kernels, fused_layer(): pl.pallas_call(functools.partial(layer_kernel, n), out_shape=jax.ShapeDty...  180 us

profile of v4, /device:TPU:0, one launch (start us, length us, event | category | flops | bytes accessed | tf_op | source)
XLA Modules:
  0.0 182.2 jit_solution(14060620346553843155)
XLA Ops:
  0.0 180.1 %shard_map.163 = bf16[384,1024]{1,0:T(8,128)(2,1)} custom-call(bf16[256,1024]{1,0:T(8,128)(2,1)} %refs_0_.1, bf16[256,1024]{1,0:T(8,128)(2,1)} %refs_1_.1, bf16[1024,256]{1,0:T(8,128)(2,1)} %refs_2_.1, bf16[256,2048]{1,0:T(8,128)(2,1)} %refs_3_.1, bf16[256,2048]{1,0:T(8,128)(2,1)} %refs_4_.1, bf16[2048,256]{1,0:T(8,128)(2,1)} %refs_5_.1, ...), custom_call_target="tpu_custom_call" | custom-call | tf_op jit(solution)/shard_map/pallas_call | solution.py:761
  180.2 2.1 %copy.19 = bf16[384,1024]{1,0:T(8,128)(2,1)} copy(bf16[384,1024]{1,0:T(8,128)(2,1)} %shard_map.163) | data formatting | bytes 1572864
